TPU v7x, 32 devices: a whole 2x2x4 slice. The times are simulated.
32 devices in a mesh: rep: 2 (over y), fs: 4 (over z), tp: 4 (over x, core).
Axes of the slice: x: 2, y: 2, z: 4, core: 2. Of those that a mesh axis runs over, the one named last changes fastest.
Arguments:
- tokens: bfloat16 [4096, 2048], P(('rep', 'fs', 'tp')), may hold values from -6 to 6
- norm_gain: float32 [2048], replicated, may hold values from 0.1 to 1.9
- w_gate: bfloat16 [2048, 3072], P('fs', 'tp'), may hold values from -0.125 to 0.125
- w_up: bfloat16 [2048, 3072], P('fs', 'tp'), may hold values from -0.125 to 0.125
- w_down: bfloat16 [3072, 2048], P('tp', 'fs'), may hold values from -0.109375 to 0.109375
- post_gain: float32 [2048], replicated, may hold values from 0.1 to 1.9
Outputs:
- result: bfloat16 [4096, 2048], P(('rep', 'fs', 'tp'))
All inputs are finite; a program needn't handle non-finite values.
Results may differ from a plain program's by a relative error of at most 0.014.
Values may be sent and summed in bfloat16 or wider, within the bound.
A program may use at most 64 MiB of HBM per device.

v0:
```python
import functools

import jax
import jax.numpy as jnp
from jax import lax
from jax.experimental import pallas as pl
from jax.experimental.pallas import tpu as pltpu
from jax.sharding import PartitionSpec as P

EPS = 1e-06
MESH = pl.DeviceIdType.MESH
PIECE = 256


def rms_scale(values, gain):
    return values * lax.rsqrt(jnp.mean(values * values, axis=-1, keepdims=True) + EPS) * gain


def plain_body(tokens, norm_gain, w_gate, w_up, w_down, post_gain):
    own_normed = rms_scale(tokens.astype(jnp.float32), norm_gain).astype(jnp.bfloat16)
    normed = lax.all_gather(own_normed, "tp", axis=0, tiled=True)
    gate = jnp.dot(
        normed, lax.all_gather(w_gate, "fs", axis=0, tiled=True), preferred_element_type=jnp.float32
    )
    up = jnp.dot(
        normed, lax.all_gather(w_up, "fs", axis=0, tiled=True), preferred_element_type=jnp.float32
    )
    hidden = (jax.nn.silu(gate) * up).astype(jnp.bfloat16)
    terms = jnp.dot(
        hidden, lax.all_gather(w_down, "fs", axis=1, tiled=True), preferred_element_type=jnp.float32
    )
    summed = lax.psum_scatter(
        terms.astype(jnp.bfloat16), "tp", scatter_dimension=0, tiled=True
    ).astype(jnp.float32)
    return rms_scale(summed, post_gain).astype(jnp.bfloat16)


def kernel(
    n, rows, depth, part, width, cuts,
    tok_ref, gain_ref, wg_ref, wu_ref, wd_ref, post_ref, out_ref,
    raw, normed, acc, gu, dn, hidden, kept, pair_out, pair_in, cross_out, cross_in, fin,
    loc_sem, tok_s, tok_r, w_s, w_r, pair_s, pair_r, cross_s, cross_r,
):
    r, k, t = lax.axis_index("rep"), lax.axis_index("fs"), lax.axis_index("tp")
    x, c = t // 2, t % 2
    t_pair, t_x, r_y = x * 2 + (1 - c), (1 - x) * 2 + c, 1 - r
    partner, along_x, along_y, diag = {"tp": t_pair}, {"tp": t_x}, {"rep": r_y}, {"rep": r_y, "tp": t_x}
    has_left, has_right = k > 0, k < n - 1

    def weight(s, q):
        if isinstance(q, int) and q < 2:
            return gu.at[s, :, pl.ds(q * part, part)]
        return dn.at[s, q - 2]

    sub = width // cuts
    half = pl.multiple_of(r * part, part)
    loads = [
        pltpu.make_async_copy(wg_ref.at[:, pl.ds(half, part)], weight(k, 0), loc_sem.at[0]),
        pltpu.make_async_copy(wu_ref.at[:, pl.ds(half, part)], weight(k, 1), loc_sem.at[1]),
        pltpu.make_async_copy(tok_ref, raw.at[pl.ds((r * 4 + t) * rows, rows)], loc_sem.at[2]),
    ] + [
        pltpu.make_async_copy(
            wd_ref.at[pl.ds(half, part), pl.ds(j * sub, sub)], dn.at[k, j], loc_sem.at[3 + j]
        )
        for j in range(cuts)
    ]
    for load in loads:
        load.start()

    barrier = pltpu.get_barrier_semaphore()
    for where in (partner, along_x, along_y, diag):
        pl.semaphore_signal(barrier, inc=1, device_id=where, device_id_type=MESH)

    @pl.when(has_left)
    def _():
        pl.semaphore_signal(barrier, inc=1, device_id={"fs": k - 1}, device_id_type=MESH)

    @pl.when(has_right)
    def _():
        pl.semaphore_signal(barrier, inc=1, device_id={"fs": k + 1}, device_id_type=MESH)

    pl.semaphore_wait(barrier, 4 + jnp.where(has_left, 1, 0) + jnp.where(has_right, 1, 0))

    def remote(ref, send, recv, where):
        return pltpu.make_async_remote_copy(ref, ref, send, recv, device_id=where, device_id_type=MESH)

    def hop(way, s, q):
        return remote(weight(s, q), w_s.at[way, s, q], w_r.at[s, q], {"fs": k + 1 - 2 * way})

    def pass_on(way, s, q):
        @pl.when(has_left if way else has_right)
        def _():
            hop(way, s, q).start()

    def rows_of(r_at, t_at, first=0, count=rows):
        return raw.at[pl.ds((r_at * 4 + t_at) * rows + first, count)]

    upper = rows // 2
    token_sends = [
        (rows_of(r, t), partner),
        (rows_of(r, t), along_x),
        (rows_of(r, t), along_y),
        (rows_of(r, t_x, 0, upper), along_y),
        (rows_of(r_y, t, upper, upper), along_x),
        (rows_of(r, t_x), partner),
        (rows_of(r_y, t), partner),
        (rows_of(r_y, t_x), partner),
    ]
    t_px = (1 - x) * 2 + (1 - c)
    token_lands = [
        rows_of(r, t_pair),
        rows_of(r, t_x),
        rows_of(r_y, t),
        rows_of(r_y, t_x, 0, upper),
        rows_of(r_y, t_x, upper, upper),
        rows_of(r, t_px),
        rows_of(r_y, t_pair),
        rows_of(r_y, t_px),
    ]

    def token_send(i):
        ref, where = token_sends[i]
        return remote(ref, tok_s.at[i], tok_r.at[i], where)

    def token_wait(i):
        remote(token_lands[i], tok_s.at[i], tok_r.at[i], partner).wait_recv()

    loads[2].wait()
    for i in (1, 2, 0):
        token_send(i).start()
    for q in (0, 1):
        loads[q].wait()
        pass_on(0, k, q)
        pass_on(1, k, q)
    for load in loads[3:]:
        load.wait()

    def start_down(step):
        for way, distance in ((0, k), (1, n - 1 - k)):
            @pl.when(distance == step)
            def _():
                for j in range(cuts):
                    pass_on(way, k, 2 + j)

    start_down(0)

    def arrive(step, q):
        for way, s in ((0, k - step), (1, k + step)):
            @pl.when((s >= 0) if way == 0 else (s < n))
            def _():
                hop(way, s, q).wait_recv()
                pass_on(way, s, q)

    def forward_tokens():
        token_wait(1)
        token_send(3).start()
        token_send(5).start()
        token_wait(2)
        token_send(4).start()
        token_send(6).start()

    def finish_tokens():
        token_wait(3)
        token_wait(4)
        token_send(7).start()
        for i in (0, 5, 6, 7):
            token_wait(i)

        tile = 32

        @pl.loop(0, 8 * rows // tile)
        def _(i):
            at = pl.ds(pl.multiple_of(i * tile, tile), tile)
            normed[at, :] = rms_scale(raw[at, :].astype(jnp.float32), gain_ref[...]).astype(jnp.bfloat16)

    tile = 2 * rows

    def add_block(s, first):
        cols = pl.ds(pl.multiple_of(s * depth, depth), depth)

        @pl.loop(0, 4)
        def _(i):
            at = pl.ds(pl.multiple_of(i * tile, tile), tile)
            term = jnp.dot(normed[at, cols], gu[s], preferred_element_type=jnp.float32)
            acc[at, :] = term if first else acc[at, :] + term

    for step in range(1, n):
        arrive(step, 0)
        if step == 1:
            forward_tokens()
        arrive(step, 1)
        start_down(step)
        if step == 1:
            finish_tokens()
            add_block(k, True)
        for s in (k - step, k + step):
            @pl.when((s >= 0) & (s < n))
            def _():
                add_block(s, False)

    @pl.loop(0, 16)
    def _(i):
        at = pl.ds(pl.multiple_of(i * (rows // 2), rows // 2), rows // 2)
        gate, up = acc[at, :part], acc[at, part:]
        hidden[at, :] = (gate / (1.0 + jnp.exp(-gate)) * up).astype(jnp.bfloat16)

    mine = r * 2 + x
    others = ((r * 2 + (1 - x), along_x), (r_y * 2 + x, along_y), (r_y * 2 + (1 - x), diag))

    def pair_copy(p):
        return pltpu.make_async_remote_copy(
            pair_out.at[p], pair_in.at[p], pair_s.at[p], pair_r.at[p], device_id=partner, device_id_type=MESH
        )

    def cross_copy(p, to, where):
        return pltpu.make_async_remote_copy(
            cross_out.at[p, to], cross_in.at[p, mine], cross_s.at[p, to], cross_r.at[p, mine],
            device_id=where, device_id_type=MESH,
        )

    both_ways = jnp.minimum(k, n - 1 - k)
    far = jnp.where(k < n - 1 - k, 1, -1)

    def source(i):
        near = jnp.where(i % 2 == 1, k - (i + 1) // 2, k + i // 2)
        return jnp.where(i <= 2 * both_ways, near, k + far * (i - both_ways))

    def product(m, core, s, j):
        at = pl.ds(pl.multiple_of((m * 2 + core) * rows, rows), rows)
        return jnp.dot(hidden[at, :], dn[s, j], preferred_element_type=jnp.float32)

    def finish(i, j, slot):
        p = source(i) * cuts + j
        pair_copy(p).wait_recv()
        for to, where in (others[2], others[0], others[1]):
            cross_out[p, to] = (kept[slot, to] + pair_in[p, to].astype(jnp.float32)).astype(jnp.bfloat16)
        for to, where in (others[2], others[0], others[1]):
            cross_copy(p, to, where).start()
        fin[p] = kept[slot, mine] + pair_in[p, mine].astype(jnp.float32)

    @pl.loop(0, n * cuts)
    def _(at):
        i, j, slot = at // cuts, at % cuts, at % 2
        s = source(i)
        p = s * cuts + j

        @pl.when(at > 0)
        def _():
            finish((at - 1) // cuts, (at - 1) % cuts, 1 - slot)

        @pl.when(i > 0)
        def _():
            remote(dn.at[s, j], w_s.at[0, s, 2 + j], w_r.at[s, 2 + j], partner).wait_recv()

        @pl.when((i > 0) & (s < k))
        def _():
            pass_on(0, s, 2 + j)

        @pl.when((i > 0) & (s > k))
        def _():
            pass_on(1, s, 2 + j)

        @pl.loop(0, 4)
        def _(m):
            pair_out[p, m] = product(m, 1 - c, s, j).astype(jnp.bfloat16)

        pair_copy(p).start()

        @pl.loop(0, 4)
        def _(m):
            kept[slot, m] = product(m, c, s, j)

    finish(n - 1, cuts - 1, (n * cuts - 1) % 2)

    for p in range(n * cuts):
        for other, _ in others:
            pltpu.make_async_remote_copy(
                cross_out.at[p, 0], cross_in.at[p, other], cross_s.at[p, 0],
                cross_r.at[p, other], device_id=along_x, device_id_type=MESH,
            ).wait_recv()

    piece = 32

    @pl.loop(0, rows // piece)
    def _(i):
        at = pl.ds(pl.multiple_of(i * piece, piece), piece)
        blocks = []
        for p in range(n * cuts):
            total = fin[p, at, :]
            for other, _ in others:
                total = total + cross_in[p, other, at, :].astype(jnp.float32)
            blocks.append(total)
        square = sum(jnp.sum(b * b, axis=-1, keepdims=True) for b in blocks)
        scale = lax.rsqrt(square / (n * width) + EPS)
        for p in range(n * cuts):
            cols = pl.ds(p * sub, sub)
            out_ref[at, cols] = (blocks[p] * scale * post_ref[:, cols]).astype(out_ref.dtype)

    for i in range(8):
        token_send(i).wait_send()
    for s in range(n):
        for q in range(2 + cuts):
            @pl.when(has_right & (s <= k))
            def _():
                hop(0, s, q).wait_send()

            @pl.when(has_left & (s >= k))
            def _():
                hop(1, s, q).wait_send()
    for p in range(n * cuts):
        pair_copy(p).wait_send()
        for to, where in others:
            cross_copy(p, to, where).wait_send()


def chain_body(n, tokens, norm_gain, w_gate, w_up, w_down, post_gain):
    rows, model = tokens.shape
    depth, block = w_gate.shape
    width = w_down.shape[1]
    part = block // 2
    cuts = max(1, width // PIECE)
    sub = width // cuts
    vmem, dma = pltpu.VMEM, pltpu.SemaphoreType.DMA
    low, full = jnp.bfloat16, jnp.float32
    anywhere = pl.BlockSpec(memory_space=pl.ANY)
    inside = pl.BlockSpec(memory_space=vmem)
    return pl.pallas_call(
        functools.partial(kernel, n, rows, depth, part, width, cuts),
        out_shape=jax.ShapeDtypeStruct((rows, model), low),
        in_specs=[anywhere, inside, anywhere, anywhere, anywhere, inside],
        out_specs=inside,
        scratch_shapes=[
            vmem((8 * rows, model), low),
            vmem((8 * rows, model), low),
            vmem((8 * rows, 2 * part), full),
            vmem((n, depth, 2 * part), low),
            vmem((n, cuts, part, sub), low),
            vmem((8 * rows, part), low),
            vmem((2, 4, rows, sub), full),
            vmem((n * cuts, 4, rows, sub), low),
            vmem((n * cuts, 4, rows, sub), low),
            vmem((n * cuts, 4, rows, sub), low),
            vmem((n * cuts, 4, rows, sub), low),
            vmem((n * cuts, rows, sub), full),
            dma((3 + cuts,)),
            dma((8,)),
            dma((8,)),
            dma((2, n, 2 + cuts)),
            dma((n, 2 + cuts)),
            dma((n * cuts,)),
            dma((n * cuts,)),
            dma((n * cuts, 4)),
            dma((n * cuts, 4)),
        ],
        compiler_params=pltpu.CompilerParams(
            collective_id=0, has_side_effects=True, vmem_limit_bytes=56 * 2**20
        ),
    )(tokens, norm_gain.reshape(1, -1), w_gate, w_up, w_down, post_gain.reshape(1, -1))


def solution(mesh):
    n = mesh.shape["fs"]

    def body(tokens, norm_gain, w_gate, w_up, w_down, post_gain):
        args = (tokens, norm_gain, w_gate, w_up, w_down, post_gain)
        rows = tokens.shape[0]
        fits = (
            mesh.shape["rep"] == 2 and mesh.shape["tp"] == 4 and 2 <= n <= 4 and rows <= 128
            and rows % 64 == 0 and w_gate.shape[1] % 256 == 0 and w_down.shape[1] % PIECE == 0
        )
        return chain_body(n, *args) if fits else plain_body(*args)

    return jax.shard_map(
        body,
        mesh=mesh,
        in_specs=(
            P(("rep", "fs", "tp"), None),
            P(),
            P("fs", "tp"),
            P("fs", "tp"),
            P("tp", "fs"),
            P(),
        ),
        out_specs=P(("rep", "fs", "tp"), None),
        check_vma=False,
    )
```

profile of v0, /device:TPU:0, one launch (start us, length us, event | category | flops | bytes accessed | tf_op | source)
XLA Modules:
  0.0 93.7 jit_solution(14161307211422612912)
XLA Ops:
  0.0 91.8 %shard_map.64 = bf16[128,2048]{1,0:T(8,128)(2,1)} custom-call(bf16[128,2048]{1,0:T(8,128)(2,1)} %tok_ref.1, f32[1,2048]{1,0:T(1,128)} %bitcast.2, bf16[512,768]{1,0:T(8,128)(2,1)} %wg_ref.1, bf16[512,768]{1,0:T(8,128)(2,1)} %wu_ref.1, bf16[768,512]{1,0:T(8,128)(2,1)} %wd_ref.1, f32[1,2048]{1,0:T(1,128)} %bitcast.3), custom_call_target="tpu_custom_call" | custom-call | tf_op jit(solution)/shard_map/pallas_call | solution.py:327
  91.8 1.9 %copy.8 = bf16[128,2048]{1,0:T(8,128)(2,1)} copy(bf16[128,2048]{1,0:T(8,128)(2,1)} %shard_map.64) | data formatting | bytes 1048576
where the time goes:
time: 94 us; the launch traced here: 93.7 us
  Pallas kernels  91.8 us (98%)
  local copies, waits for them, and re-layouts  1.88 us (2%)
    pallas_call x1, Pallas kernels, chain_body(): pl.pallas_call(functools.partial(kernel, n, rows, depth, part, width, cut...  91.8 us
    unnamed x1, local copies, waits for them, and re-layouts  1.88 us

commit v1 on v0

v1 whole, which is shorter than its diff:
```python
import functools

import jax
import jax.numpy as jnp
from jax import lax
from jax.experimental import pallas as pl
from jax.experimental.pallas import tpu as pltpu
from jax.sharding import PartitionSpec as P

EPS = 1e-06
MESH = pl.DeviceIdType.MESH
PIECE = 256
LANES = 128


def rms_scale(values, gain):
    return values * lax.rsqrt(jnp.mean(values * values, axis=-1, keepdims=True) + EPS) * gain


def plain_body(tokens, norm_gain, w_gate, w_up, w_down, post_gain):
    own_normed = rms_scale(tokens.astype(jnp.float32), norm_gain).astype(jnp.bfloat16)
    normed = lax.all_gather(own_normed, "tp", axis=0, tiled=True)
    gate = jnp.dot(
        normed, lax.all_gather(w_gate, "fs", axis=0, tiled=True), preferred_element_type=jnp.float32
    )
    up = jnp.dot(
        normed, lax.all_gather(w_up, "fs", axis=0, tiled=True), preferred_element_type=jnp.float32
    )
    hidden = (jax.nn.silu(gate) * up).astype(jnp.bfloat16)
    terms = jnp.dot(
        hidden, lax.all_gather(w_down, "fs", axis=1, tiled=True), preferred_element_type=jnp.float32
    )
    summed = lax.psum_scatter(
        terms.astype(jnp.bfloat16), "tp", scatter_dimension=0, tiled=True
    ).astype(jnp.float32)
    return rms_scale(summed, post_gain).astype(jnp.bfloat16)


def kernel(
    n, rows, depth, part, width, cuts, lanes,
    tok_ref, gain_ref, wg_ref, wu_ref, wd_ref, post_ref, out_ref,
    raw, tok, gu, dn, hid, hdel, kept, pair_out, pair_in, cross_out, cross_in, fin,
    tok_l, gu_l, dn_l, z_s, z_r, tok_s, tok_r, gu_s, gu_r, dn_s, dn_r, hid_s, hid_r,
    pair_s, pair_r, cross_s, cross_r,
):
    r, k, t = lax.axis_index("rep"), lax.axis_index("fs"), lax.axis_index("tp")
    x, c = t // 2, t % 2
    t_pair, t_x, r_y = x * 2 + (1 - c), (1 - x) * 2 + c, 1 - r
    t_px = (1 - x) * 2 + (1 - c)
    partner, along_x, along_y, diag = {"tp": t_pair}, {"tp": t_x}, {"rep": r_y}, {"rep": r_y, "tp": t_x}
    left = k < n // 2
    last = jnp.where(left, 0, n - 1)
    near = jnp.where(left, 1, n - 2)
    far_near, far_last = n - 1 - near, n - 1 - last
    at_end = k == last
    in_middle = k != last
    inner, outer = {"fs": jnp.where(left, k + 1, k - 1)}, {"fs": last}
    blocks = part // lanes
    sub = width // cuts
    half = pl.multiple_of(r * part, part)
    halves = rows // 2

    def gu_load(b, q):
        ref = (wg_ref, wu_ref)[q]
        at = pl.ds(pl.multiple_of(k * depth, depth), depth)
        return pltpu.make_async_copy(
            ref.at[:, pl.ds(half + b * lanes, lanes)], gu.at[b, at, pl.ds(q * lanes, lanes)], gu_l.at[b, q]
        )

    def dn_load(j):
        return pltpu.make_async_copy(
            wd_ref.at[pl.ds(half, part), pl.ds(j * sub, sub)], dn.at[k, j], dn_l.at[j]
        )

    tok_load = pltpu.make_async_copy(tok_ref, raw, tok_l)

    tok_load.start()
    for b in range(blocks):
        for q in (0, 1):
            gu_load(b, q).start()
    for j in range(cuts):
        dn_load(j).start()

    barrier = pltpu.get_barrier_semaphore()
    for where in (partner, along_x, along_y, diag, inner):
        pl.semaphore_signal(barrier, inc=1, device_id=where, device_id_type=MESH)

    @pl.when(in_middle)
    def _():
        pl.semaphore_signal(barrier, inc=1, device_id=outer, device_id_type=MESH)

    pl.semaphore_wait(barrier, 5 + jnp.where(in_middle, 1, 0))

    def remote(ref, send, recv, where, to=None):
        return pltpu.make_async_remote_copy(
            ref, ref if to is None else to, send, recv, device_id=where, device_id_type=MESH
        )

    def gu_at(s, b):
        return gu.at[b, pl.ds(pl.multiple_of(s * depth, depth), depth)]

    def gu_send(kind, b):
        s = last if kind else k
        return remote(gu_at(s, b), gu_s.at[kind, b], gu_r.at[s, b], inner)

    def gu_wait(s, b):
        remote(gu_at(s, b), gu_s.at[0, b], gu_r.at[s, b], inner).wait_recv()

    def dn_send(way, s, j):
        return remote(dn.at[s, j], dn_s.at[way, s, j], dn_r.at[s, j], outer if way else inner)

    def dn_wait(s, j):
        remote(dn.at[s, j], dn_s.at[0, s, j], dn_r.at[s, j], inner).wait_recv()

    def rows_of(p, r_at, t_at, h):
        return tok.at[p, pl.ds((r_at * 4 + t_at) * rows + h * halves, halves)]

    def z_send(h):
        return remote(rows_of(0, r, t, h), z_s.at[h], z_r.at[h], inner, rows_of(1, r, t, h))

    def z_wait(h):
        remote(rows_of(1, r, t, h), z_s.at[h], z_r.at[h], inner).wait_recv()

    U, L = 0, 1
    sends = [
        ((r, t, U), along_x), ((r, t, L), along_x), ((r, t, U), along_y), ((r, t, L), along_y),
        ((r, t_x, U), along_y), ((r_y, t, L), along_x),
        ((r, t, U), partner), ((r, t, L), partner),
        ((r, t_x, U), partner), ((r, t_x, L), partner),
        ((r_y, t, U), partner), ((r_y, t, L), partner),
        ((r_y, t_x, U), partner), ((r_y, t_x, L), partner),
    ]
    lands = [
        (r, t_x, U), (r, t_x, L), (r_y, t, U), (r_y, t, L),
        (r_y, t_x, U), (r_y, t_x, L),
        (r, t_pair, U), (r, t_pair, L),
        (r, t_px, U), (r, t_px, L),
        (r_y, t_pair, U), (r_y, t_pair, L),
        (r_y, t_px, U), (r_y, t_px, L),
    ]

    def tok_send(p, i):
        at, where = sends[i]
        return remote(rows_of(p, *at), tok_s.at[p, i], tok_r.at[p, i], where)

    def go(p, *which):
        for i in which:
            tok_send(p, i).start()

    def got(p, *which):
        for i in which:
            remote(rows_of(p, *lands[i]), tok_s.at[p, i], tok_r.at[p, i], partner).wait_recv()

    quarter = 2 * rows

    def hid_send(b, m):
        at = (pl.ds(pl.multiple_of(m * quarter, quarter), quarter), pl.ds(b * lanes, lanes))
        return remote(hdel.at[at], hid_s.at[b, m], hid_r.at[b, m], outer, hid.at[at])

    def hid_wait(b, m):
        at = (pl.ds(pl.multiple_of(m * quarter, quarter), quarter), pl.ds(b * lanes, lanes))
        remote(hid.at[at], hid_s.at[b, m], hid_r.at[b, m], partner).wait_recv()

    def gated(p, b, m):
        at = pl.ds(pl.multiple_of(m * quarter, quarter), quarter)
        both = jnp.dot(tok[p, at, :], gu[b], preferred_element_type=jnp.float32)
        gate, up = both[:, :lanes], both[:, lanes:]
        value = (gate / (1.0 + jnp.exp(-gate)) * up).astype(jnp.bfloat16)
        (hdel if p else hid)[at, pl.ds(b * lanes, lanes)] = value

    def own_block(b):
        @pl.loop(0, 4)
        def _(m):
            gated(0, b, m)

    def passed_block(b):
        @pl.loop(0, 4)
        def _(m):
            gated(1, b, m)
            hid_send(b, m).start()

    def send_own_gu():
        for b in range(blocks):
            gu_load(b, 0).wait()
            gu_load(b, 1).wait()
            gu_send(0, b).start()

    @pl.when(in_middle)
    def _():
        send_own_gu()
        for j in range(cuts):
            dn_load(j).wait()
            dn_send(1, k, j).start()

    tok_load.wait()
    tile = 32
    first = (r * 4 + t) * rows

    @pl.loop(0, rows // tile)
    def _(i):
        at = pl.ds(pl.multiple_of(i * tile, tile), tile)
        to = pl.ds(pl.multiple_of(first + i * tile, tile), tile)
        tok[0, to, :] = rms_scale(raw[at, :].astype(jnp.float32), gain_ref[...]).astype(jnp.bfloat16)

    @pl.when(at_end)
    def _():
        z_send(U).start()
        z_send(L).start()
        send_own_gu()
        for j in range(cuts):
            dn_load(j).wait()
            dn_send(0, k, j).start()

    @pl.when(in_middle)
    def _():
        go(0, 0, 2, 6, 7)
        z_wait(U)
        go(1, 0, 2, 6)
        got(0, 0)
        go(0, 8)
        got(0, 2)
        go(0, 10)
        z_wait(L)
        go(1, 1, 3, 7)
        got(1, 0)
        go(1, 4, 8)
        got(1, 2)
        go(1, 10)
        gu_wait(last, 0)
        gu_send(1, 0).start()
        got(1, 3)
        go(1, 5, 11)
        got(1, 1)
        go(1, 9)
        go(0, 1, 3, 4)
        for b in range(1, blocks - 1):
            gu_wait(last, b)
            gu_send(1, b).start()
        got(1, 4)
        go(1, 12)
        got(1, 5)
        go(1, 13)
        got(1, 6, 7, 8, 9, 10, 11, 12, 13)
        for b in range(blocks - 1):
            gu_wait(far_near, b)
            gu_wait(far_last, b)
            passed_block(b)
            if b == 0:
                gu_wait(last, blocks - 1)
                gu_send(1, blocks - 1).start()
                for j in range(cuts):
                    dn_send(0, k, j).start()
        got(0, 3)
        go(0, 5, 11)
        got(0, 1)
        go(0, 9)
        got(0, 4)
        go(0, 12)
        got(0, 5)
        go(0, 13)
        got(0, 6, 7, 8, 9, 10, 11, 12, 13)
        for b in range(blocks - 1):
            own_block(b)
        gu_wait(far_near, blocks - 1)
        gu_wait(far_last, blocks - 1)
        passed_block(blocks - 1)
        own_block(blocks - 1)

    mine = r * 2 + x
    others = ((r * 2 + (1 - x), along_x), (r_y * 2 + x, along_y), (r_y * 2 + (1 - x), diag))

    def pair_copy(p):
        return pltpu.make_async_remote_copy(
            pair_out.at[p], pair_in.at[p], pair_s.at[p], pair_r.at[p], device_id=partner, device_id_type=MESH
        )

    def cross_copy(p, to, where):
        return pltpu.make_async_remote_copy(
            cross_out.at[p, to], cross_in.at[p, mine], cross_s.at[p, to], cross_r.at[p, mine],
            device_id=where, device_id_type=MESH,
        )

    def source(i):
        near_or_last = jnp.where(i == 0, k, near + last - k)
        return jnp.where(i < 2, near_or_last, jnp.where(i == 2, far_near, far_last))

    def product(m, core, s, j):
        at = pl.ds(pl.multiple_of((m * 2 + core) * rows, rows), rows)
        return jnp.dot(hid[at, :], dn[s, j], preferred_element_type=jnp.float32)

    def finish(i, j, slot):
        p = source(i) * cuts + j
        pair_copy(p).wait_recv()
        for to, where in (others[2], others[0], others[1]):
            cross_out[p, to] = (kept[slot, to] + pair_in[p, to].astype(jnp.float32)).astype(jnp.bfloat16)
        for to, where in (others[2], others[0], others[1]):
            cross_copy(p, to, where).start()
        fin[p] = kept[slot, mine] + pair_in[p, mine].astype(jnp.float32)

    @pl.loop(0, n * cuts)
    def _(at):
        i, j, slot = at // cuts, at % cuts, at % 2
        s = source(i)
        p = s * cuts + j

        @pl.when(at > 0)
        def _():
            finish((at - 1) // cuts, (at - 1) % cuts, 1 - slot)

        @pl.when(i > 0)
        def _():
            dn_wait(s, j)

        @pl.when((i == 1) & in_middle)
        def _():
            dn_send(0, s, j).start()

        @pl.when((i > 1) & in_middle)
        def _():
            dn_send(1, s, j).start()

        @pl.loop(0, 4)
        def _(m):
            @pl.when((at == 0) & at_end)
            def _():
                for b in range(blocks):
                    hid_wait(b, m)

            pair_out[p, m] = product(m, 1 - c, s, j).astype(jnp.bfloat16)

        pair_copy(p).start()

        @pl.loop(0, 4)
        def _(m):
            kept[slot, m] = product(m, c, s, j)

    finish(n - 1, cuts - 1, (n * cuts - 1) % 2)

    for p in range(n * cuts):
        for other, _ in others:
            pltpu.make_async_remote_copy(
                cross_out.at[p, 0], cross_in.at[p, other], cross_s.at[p, 0],
                cross_r.at[p, other], device_id=along_x, device_id_type=MESH,
            ).wait_recv()

    piece = 32

    @pl.loop(0, rows // piece)
    def _(i):
        at = pl.ds(pl.multiple_of(i * piece, piece), piece)
        parts = []
        for p in range(n * cuts):
            total = fin[p, at, :]
            for other, _ in others:
                total = total + cross_in[p, other, at, :].astype(jnp.float32)
            parts.append(total)
        square = sum(jnp.sum(b * b, axis=-1, keepdims=True) for b in parts)
        scale = lax.rsqrt(square / (n * width) + EPS)
        for p in range(n * cuts):
            cols = pl.ds(p * sub, sub)
            out_ref[at, cols] = (parts[p] * scale * post_ref[:, cols]).astype(out_ref.dtype)

    for b in range(blocks):
        gu_send(0, b).wait_send()

    @pl.when(at_end)
    def _():
        z_send(U).wait_send()
        z_send(L).wait_send()
        for j in range(cuts):
            dn_send(0, k, j).wait_send()

    @pl.when(in_middle)
    def _():
        for p in (0, 1):
            for i in range(len(sends)):
                tok_send(p, i).wait_send()
        for b in range(blocks):
            gu_send(1, b).wait_send()
            for m in range(4):
                hid_send(b, m).wait_send()
        for j in range(cuts):
            dn_send(0, k, j).wait_send()
            dn_send(0, last, j).wait_send()
            dn_send(1, k, j).wait_send()
            dn_send(1, far_near, j).wait_send()
            dn_send(1, far_last, j).wait_send()

    for p in range(n * cuts):
        pair_copy(p).wait_send()
        for to, where in others:
            cross_copy(p, to, where).wait_send()


def chain_body(n, tokens, norm_gain, w_gate, w_up, w_down, post_gain):
    rows, model = tokens.shape
    depth, block = w_gate.shape
    width = w_down.shape[1]
    part = block // 2
    cuts = max(1, width // PIECE)
    sub = width // cuts
    blocks = part // LANES
    vmem, dma = pltpu.VMEM, pltpu.SemaphoreType.DMA
    low, full = jnp.bfloat16, jnp.float32
    anywhere = pl.BlockSpec(memory_space=pl.ANY)
    inside = pl.BlockSpec(memory_space=vmem)
    return pl.pallas_call(
        functools.partial(kernel, n, rows, depth, part, width, cuts, LANES),
        out_shape=jax.ShapeDtypeStruct((rows, model), low),
        in_specs=[anywhere, inside, anywhere, anywhere, anywhere, inside],
        out_specs=inside,
        scratch_shapes=[
            vmem((rows, model), low),
            vmem((2, 8 * rows, model), low),
            vmem((blocks, n * depth, 2 * LANES), low),
            vmem((n, cuts, part, sub), low),
            vmem((8 * rows, part), low),
            vmem((8 * rows, part), low),
            vmem((2, 4, rows, sub), full),
            vmem((n * cuts, 4, rows, sub), low),
            vmem((n * cuts, 4, rows, sub), low),
            vmem((n * cuts, 4, rows, sub), low),
            vmem((n * cuts, 4, rows, sub), low),
            vmem((n * cuts, rows, sub), full),
            dma(()),
            dma((blocks, 2)),
            dma((cuts,)),
            dma((2,)),
            dma((2,)),
            dma((2, 14)),
            dma((2, 14)),
            dma((2, blocks)),
            dma((n, blocks)),
            dma((2, n, cuts)),
            dma((n, cuts)),
            dma((blocks, 4)),
            dma((blocks, 4)),
            dma((n * cuts,)),
            dma((n * cuts,)),
            dma((n * cuts, 4)),
            dma((n * cuts, 4)),
        ],
        compiler_params=pltpu.CompilerParams(
            collective_id=0, has_side_effects=True, vmem_limit_bytes=56 * 2**20
        ),
    )(tokens, norm_gain.reshape(1, -1), w_gate, w_up, w_down, post_gain.reshape(1, -1))


def solution(mesh):
    n = mesh.shape["fs"]

    def body(tokens, norm_gain, w_gate, w_up, w_down, post_gain):
        args = (tokens, norm_gain, w_gate, w_up, w_down, post_gain)
        rows = tokens.shape[0]
        fits = (
            mesh.shape["rep"] == 2 and mesh.shape["tp"] == 4 and n == 4 and rows <= 128
            and rows % 64 == 0 and w_gate.shape[1] % 256 == 0 and w_down.shape[1] % PIECE == 0
        )
        return chain_body(n, *args) if fits else plain_body(*args)

    return jax.shard_map(
        body,
        mesh=mesh,
        in_specs=(
            P(("rep", "fs", "tp"), None),
            P(),
            P("fs", "tp"),
            P("fs", "tp"),
            P("tp", "fs"),
            P(),
        ),
        out_specs=P(("rep", "fs", "tp"), None),
        check_vma=False,
    )
```

time: 94 us -> 94.1 us (level)
  no operation moved by 1% of the time
where the time goes in v1:
time: 94.1 us; the launch traced here: 93.8 us
  Pallas kernels  92 us (98%)
  local copies, waits for them, and re-layouts  1.88 us (2%)
    pallas_call x1, Pallas kernels, chain_body(): pl.pallas_call(functools.partial(kernel, n, rows, depth, part, width, cut...  92 us

profile of v1, /device:TPU:0, one launch (start us, length us, event | category | flops | bytes accessed | tf_op | source)
XLA Modules:
  0.0 93.8 jit_solution(4357335357618734875)
XLA Ops:
  0.0 92.0 %shard_map.64 = bf16[128,2048]{1,0:T(8,128)(2,1)} custom-call(bf16[128,2048]{1,0:T(8,128)(2,1)} %tok_ref.1, f32[1,2048]{1,0:T(1,128)} %bitcast.2, bf16[512,768]{1,0:T(8,128)(2,1)} %wg_ref.1, bf16[512,768]{1,0:T(8,128)(2,1)} %wu_ref.1, bf16[768,512]{1,0:T(8,128)(2,1)} %wd_ref.1, f32[1,2048]{1,0:T(1,128)} %bitcast.3), custom_call_target="tpu_custom_call" | custom-call | tf_op jit(solution)/shard_map/pallas_call | solution.py:407
  92.0 1.9 %copy.8 = bf16[128,2048]{1,0:T(8,128)(2,1)} copy(bf16[128,2048]{1,0:T(8,128)(2,1)} %shard_map.64) | data formatting | bytes 1048576

commit v2 on v1

v2 whole, which is shorter than its diff:
```python
import functools

import jax
import jax.numpy as jnp
from jax import lax
from jax.experimental import pallas as pl
from jax.experimental.pallas import tpu as pltpu
from jax.sharding import PartitionSpec as P

EPS = 1e-06
MESH = pl.DeviceIdType.MESH
PIECE = 256
LANES = 128


def rms_scale(values, gain):
    return values * lax.rsqrt(jnp.mean(values * values, axis=-1, keepdims=True) + EPS) * gain


def plain_body(tokens, norm_gain, w_gate, w_up, w_down, post_gain):
    own_normed = rms_scale(tokens.astype(jnp.float32), norm_gain).astype(jnp.bfloat16)
    normed = lax.all_gather(own_normed, "tp", axis=0, tiled=True)
    gate = jnp.dot(
        normed, lax.all_gather(w_gate, "fs", axis=0, tiled=True), preferred_element_type=jnp.float32
    )
    up = jnp.dot(
        normed, lax.all_gather(w_up, "fs", axis=0, tiled=True), preferred_element_type=jnp.float32
    )
    hidden = (jax.nn.silu(gate) * up).astype(jnp.bfloat16)
    terms = jnp.dot(
        hidden, lax.all_gather(w_down, "fs", axis=1, tiled=True), preferred_element_type=jnp.float32
    )
    summed = lax.psum_scatter(
        terms.astype(jnp.bfloat16), "tp", scatter_dimension=0, tiled=True
    ).astype(jnp.float32)
    return rms_scale(summed, post_gain).astype(jnp.bfloat16)


def kernel(
    n, rows, depth, part, width, cuts, lanes,
    tok_ref, gain_ref, wg_ref, wu_ref, wd_ref, post_ref, out_ref,
    raw, tok, gu, dn, hid, hdel, kept, pair_out, pair_in, half_out, half_in, full_out, full_in, fin, squares,
    tok_l, gu_l, dn_l, z_s, z_r, tok_s, tok_r, gu_s, gu_r, dn_s, dn_r, hid_s, hid_r,
    pair_s, pair_r, half_s, half_r, full_s, full_r,
):
    r, k, t = lax.axis_index("rep"), lax.axis_index("fs"), lax.axis_index("tp")
    x, c = t // 2, t % 2
    t_pair, t_x, r_y = x * 2 + (1 - c), (1 - x) * 2 + c, 1 - r
    t_px = (1 - x) * 2 + (1 - c)
    partner, along_x, along_y, diag = {"tp": t_pair}, {"tp": t_x}, {"rep": r_y}, {"rep": r_y, "tp": t_x}
    left = k < n // 2
    last = jnp.where(left, 0, n - 1)
    near = jnp.where(left, 1, n - 2)
    far_near, far_last = n - 1 - near, n - 1 - last
    at_end = k == last
    in_middle = k != last
    inner, outer = {"fs": jnp.where(left, k + 1, k - 1)}, {"fs": last}
    blocks = part // lanes
    sub = width // cuts
    half = pl.multiple_of(r * part, part)
    piece = rows // 4

    def gu_load(b, q):
        ref = (wg_ref, wu_ref)[q]
        at = pl.ds(pl.multiple_of(k * depth, depth), depth)
        return pltpu.make_async_copy(
            ref.at[:, pl.ds(half + b * lanes, lanes)], gu.at[b, at, pl.ds(q * lanes, lanes)], gu_l.at[b, q]
        )

    def dn_load(j):
        return pltpu.make_async_copy(
            wd_ref.at[pl.ds(half, part), pl.ds(j * sub, sub)], dn.at[k, j], dn_l.at[j]
        )

    tok_load = pltpu.make_async_copy(tok_ref, raw, tok_l)

    tok_load.start()
    for b in range(blocks):
        for q in (0, 1):
            gu_load(b, q).start()
    for j in range(cuts):
        dn_load(j).start()

    barrier = pltpu.get_barrier_semaphore()
    for where in (partner, along_x, along_y, diag, inner):
        pl.semaphore_signal(barrier, inc=1, device_id=where, device_id_type=MESH)

    @pl.when(in_middle)
    def _():
        pl.semaphore_signal(barrier, inc=1, device_id=outer, device_id_type=MESH)

    pl.semaphore_wait(barrier, 5 + jnp.where(in_middle, 1, 0))

    def remote(ref, send, recv, where, to=None):
        return pltpu.make_async_remote_copy(
            ref, ref if to is None else to, send, recv, device_id=where, device_id_type=MESH
        )

    def gu_at(s, b):
        return gu.at[b, pl.ds(pl.multiple_of(s * depth, depth), depth)]

    def gu_send(kind, b):
        s = last if kind else k
        return remote(gu_at(s, b), gu_s.at[kind, b], gu_r.at[s, b], inner)

    def gu_wait(s, b):
        remote(gu_at(s, b), gu_s.at[0, b], gu_r.at[s, b], inner).wait_recv()

    def dn_send(way, s, j):
        return remote(dn.at[s, j], dn_s.at[way, s, j], dn_r.at[s, j], outer if way else inner)

    def dn_wait(s, j):
        remote(dn.at[s, j], dn_s.at[0, s, j], dn_r.at[s, j], inner).wait_recv()

    def rows_of(p, r_at, t_at, first, count):
        base = ((t_at % 2) * 4 + r_at * 2 + t_at // 2) * rows
        return tok.at[p, pl.ds(base + first * piece, count * piece)]

    def z_send(i):
        return remote(rows_of(0, r, t, i, 1), z_s.at[i], z_r.at[i], inner, rows_of(1, r, t, i, 1))

    def z_wait(i):
        remote(rows_of(1, r, t, i, 1), z_s.at[i], z_r.at[i], inner).wait_recv()

    sends = (
        [((r, t, i, 1), along_x) for i in range(4)]
        + [((r, t, i, 1), along_y) for i in range(4)]
        + [((r, t_x, 0, 1), along_y), ((r, t_x, 1, 1), along_y), ((r_y, t, 2, 1), along_x), ((r_y, t, 3, 1), along_x)]
        + [((r_at, t_at, i, 2), partner) for r_at, t_at in ((r, t), (r, t_x), (r_y, t), (r_y, t_x)) for i in (0, 2)]
    )
    lands = (
        [(r, t_x, i, 1) for i in range(4)]
        + [(r_y, t, i, 1) for i in range(4)]
        + [(r_y, t_x, i, 1) for i in range(4)]
        + [(r_at, t_at, i, 2) for r_at, t_at in ((r, t_pair), (r, t_px), (r_y, t_pair), (r_y, t_px)) for i in (0, 2)]
    )

    def tok_send(p, i):
        at, where = sends[i]
        return remote(rows_of(p, *at), tok_s.at[p, i], tok_r.at[p, i], where)

    def go(p, *which):
        for i in which:
            tok_send(p, i).start()

    def got(p, *which):
        for i in which:
            remote(rows_of(p, *lands[i]), tok_s.at[p, i], tok_r.at[p, i], partner).wait_recv()

    quarter = 2 * rows

    def hid_send(b, m):
        at = (pl.ds(pl.multiple_of(m * quarter, quarter), quarter), pl.ds(b * lanes, lanes))
        return remote(hdel.at[at], hid_s.at[b, m], hid_r.at[b, m], outer, hid.at[at])

    def hid_wait(b, m):
        at = (pl.ds(pl.multiple_of(m * quarter, quarter), quarter), pl.ds(b * lanes, lanes))
        remote(hid.at[at], hid_s.at[b, m], hid_r.at[b, m], partner).wait_recv()

    def gated(p, b, m):
        at = pl.ds(pl.multiple_of(m * quarter, quarter), quarter)
        both = jnp.dot(tok[p, at, :], gu[b], preferred_element_type=jnp.float32)
        gate, up = both[:, :lanes], both[:, lanes:]
        value = (gate / (1.0 + jnp.exp(-gate)) * up).astype(jnp.bfloat16)
        (hdel if p else hid)[at, pl.ds(b * lanes, lanes)] = value

    def own_block(b, r_at):
        @pl.loop(0, 2)
        def _(i):
            gated(0, b, i * 2 + r_at)

    def passed_block(b):
        @pl.loop(0, 4)
        def _(i):
            m = ((1 - c) * 2 + i) % 4
            gated(1, b, m)
            hid_send(b, m).start()

    def send_own_gu():
        for b in range(blocks):
            gu_load(b, 0).wait()
            gu_load(b, 1).wait()
            gu_send(0, b).start()

    @pl.when(in_middle)
    def _():
        send_own_gu()
        for j in range(cuts):
            dn_load(j).wait()
            dn_send(1, k, j).start()

    tok_load.wait()
    tile = 32
    first = (c * 4 + r * 2 + x) * rows

    @pl.loop(0, rows // tile)
    def _(i):
        at = pl.ds(pl.multiple_of(i * tile, tile), tile)
        to = pl.ds(pl.multiple_of(first + i * tile, tile), tile)
        tok[0, to, :] = rms_scale(raw[at, :].astype(jnp.float32), gain_ref[...]).astype(jnp.bfloat16)

    @pl.when(at_end)
    def _():
        for i in range(4):
            z_send(i).start()
        send_own_gu()
        for j in range(cuts):
            dn_load(j).wait()
            dn_send(0, k, j).start()

    @pl.when(in_middle)
    def _():
        go(0, 0, 1, 6, 7, 12, 13)
        z_wait(0)
        go(1, 0, 4)
        got(0, 0, 1)
        go(0, 14)
        got(0, 6, 7)
        go(0, 17)
        z_wait(1)
        go(1, 1, 5, 12)
        got(1, 0, 4)
        z_wait(2)
        go(1, 2, 6)
        got(1, 1, 5)
        go(1, 14, 16)
        z_wait(3)
        go(1, 3, 7, 13, 8, 9)
        got(1, 6)
        go(1, 10)
        got(1, 7)
        go(1, 11, 17)
        got(1, 2, 3)
        go(1, 15)
        go(0, 2, 3, 4, 5, 8, 9, 10, 11)
        gu_wait(last, 0)
        gu_send(1, 0).start()
        gu_wait(last, 1)
        gu_send(1, 1).start()
        got(1, 8, 9)
        go(1, 18)
        got(1, 10, 11)
        go(1, 19)
        got(1, 12, 13, 14, 15, 16, 17, 18, 19)
        gu_wait(far_near, 0)
        gu_wait(far_last, 0)
        passed_block(0)
        got(0, 2, 3)
        go(0, 15)
        got(0, 4, 5)
        go(0, 16)
        gu_wait(last, 2)
        gu_send(1, 2).start()
        gu_wait(far_near, 1)
        gu_wait(far_last, 1)
        passed_block(1)
        got(0, 12, 13, 14, 15)
        own_block(0, r)
        own_block(1, r)
        dn_wait(last, 0)
        got(0, 8, 9)
        go(0, 18)
        got(0, 10, 11)
        go(0, 19)
        gu_wait(far_near, 2)
        gu_wait(far_last, 2)
        for j in range(cuts):
            dn_send(0, k, j).start()
        dn_send(0, last, 0).start()
        passed_block(2)
        dn_wait(last, 1)
        dn_send(0, last, 1).start()
        own_block(2, r)
        got(0, 16, 17, 18, 19)
        own_block(0, r_y)
        own_block(1, r_y)
        dn_wait(far_near, 0)
        dn_send(1, far_near, 0).start()
        own_block(2, r_y)

    mine, at_x, at_y, at_diag = r * 2 + x, r * 2 + (1 - x), r_y * 2 + x, r_y * 2 + (1 - x)
    chunks = n * cuts
    slots = 2
    mid = sub // 2

    def of(m):
        return pl.ds(pl.multiple_of(m * rows, rows), rows)

    def pair_copy(p):
        return remote(pair_out.at[p], pair_s.at[p], pair_r.at[p], partner, pair_in.at[p])

    def half_copy(p, way):
        return remote(
            half_out.at[p, way], half_s.at[p, way], half_r.at[p, way], along_y if way else along_x, half_in.at[p, way]
        )

    def full_copy(p, way):
        return remote(
            full_out.at[p, way], full_s.at[p, way], full_r.at[p, way], along_y if way else along_x, full_in.at[p, way]
        )

    def source(i):
        near_or_last = jnp.where(i == 0, k, near + last - k)
        return jnp.where(i < 2, near_or_last, jnp.where(i == 2, far_near, far_last))

    def place(at):
        return source(at // cuts) * cuts + at % cuts

    def product(core, s, j):
        at = pl.ds(pl.multiple_of(core * 4 * rows, 4 * rows), 4 * rows)
        return jnp.dot(hid[at, :], dn[s, j], preferred_element_type=jnp.float32)

    def finish_pair(at):
        p, slot = place(at), at % slots
        pair_copy(p).wait_recv()

        def summed(m):
            return kept[slot, of(m), :] + pair_in[p, of(m), :].astype(jnp.float32)

        across = summed(at_diag).astype(jnp.bfloat16)
        half_out[p, 0] = across[:, :mid]
        half_out[p, 1] = across[:, mid:]
        half_copy(p, 0).start()
        half_copy(p, 1).start()
        kept[slot, of(at_x), :] = summed(at_x)
        kept[slot, of(at_y), :] = summed(at_y)
        fin[p] = summed(mine)

    def finish_half(at):
        p, slot = place(at), at % slots
        half_copy(p, 1).wait_recv()
        full_out[p, 0, :, :mid] = kept[slot, of(at_x), :mid].astype(jnp.bfloat16)
        full_out[p, 0, :, mid:] = (kept[slot, of(at_x), mid:] + half_in[p, 1].astype(jnp.float32)).astype(jnp.bfloat16)
        full_copy(p, 0).start()
        half_copy(p, 0).wait_recv()
        full_out[p, 1, :, mid:] = kept[slot, of(at_y), mid:].astype(jnp.bfloat16)
        full_out[p, 1, :, :mid] = (kept[slot, of(at_y), :mid] + half_in[p, 0].astype(jnp.float32)).astype(jnp.bfloat16)
        full_copy(p, 1).start()

    def pass_down(s, j):
        dn_wait(s, j)
        dn_send(1, s, j).start()

    @pl.loop(0, chunks)
    def _(at):
        i, j, slot = at // cuts, at % cuts, at % slots
        s = source(i)
        p = s * cuts + j

        for step, (from_s, from_j) in ((1, (far_near, 1)), (2, (far_last, 0)), (4, (far_last, 1))):
            @pl.when(in_middle & (at == step))
            def _():
                pass_down(from_s, from_j)

        @pl.when((i > 0) & at_end)
        def _():
            dn_wait(s, j)

        def arrived(core):
            @pl.when((at == 0) & at_end)
            def _():
                for b in range(blocks):
                    for half_at in (0, 1):
                        hid_wait(b, core * 2 + half_at)

        arrived(1 - c)
        pair_out[p] = product(1 - c, s, j).astype(jnp.bfloat16)
        pair_copy(p).start()
        arrived(c)
        kept[slot] = product(c, s, j)
        finish_pair(at)

        @pl.when(at > 0)
        def _():
            finish_half(at - 1)

    finish_half(chunks - 1)

    for b in range(blocks):
        gu_send(0, b).wait_send()

    @pl.when(at_end)
    def _():
        for i in range(4):
            z_send(i).wait_send()
        for j in range(cuts):
            dn_send(0, k, j).wait_send()

    @pl.when(in_middle)
    def _():
        for p in (0, 1):
            for i in range(len(sends)):
                tok_send(p, i).wait_send()
        for b in range(blocks):
            gu_send(1, b).wait_send()
            for m in range(4):
                hid_send(b, m).wait_send()
        for j in range(cuts):
            dn_send(0, k, j).wait_send()
            dn_send(0, last, j).wait_send()
            dn_send(1, k, j).wait_send()
            dn_send(1, far_near, j).wait_send()
            dn_send(1, far_last, j).wait_send()

    for p in range(chunks):
        pair_copy(p).wait_send()
        for way in (0, 1):
            half_copy(p, way).wait_send()

    squares[...] = jnp.zeros_like(squares)

    @pl.loop(0, chunks)
    def _(at):
        p = place(at)
        for way in (0, 1):
            full_copy(p, way).wait_send()
            full_copy(p, way).wait_recv()
        total = fin[p] + full_in[p, 0].astype(jnp.float32) + full_in[p, 1].astype(jnp.float32)
        fin[p] = total
        squares[...] += total[:, :mid] * total[:, :mid] + total[:, mid:] * total[:, mid:]

    scale = lax.rsqrt(jnp.sum(squares[...], axis=-1, keepdims=True) / (n * width) + EPS)
    for p in range(chunks):
        cols = pl.ds(p * sub, sub)
        out_ref[:, cols] = (fin[p] * scale * post_ref[:, cols]).astype(out_ref.dtype)


def chain_body(n, tokens, norm_gain, w_gate, w_up, w_down, post_gain):
    rows, model = tokens.shape
    depth, block = w_gate.shape
    width = w_down.shape[1]
    part = block // 2
    cuts = max(1, width // PIECE)
    sub = width // cuts
    blocks = part // LANES
    vmem, dma = pltpu.VMEM, pltpu.SemaphoreType.DMA
    low, full = jnp.bfloat16, jnp.float32
    anywhere = pl.BlockSpec(memory_space=pl.ANY)
    inside = pl.BlockSpec(memory_space=vmem)
    return pl.pallas_call(
        functools.partial(kernel, n, rows, depth, part, width, cuts, LANES),
        out_shape=pltpu.VMEM((rows, model), low),
        in_specs=[anywhere, inside, anywhere, anywhere, anywhere, inside],
        out_specs=inside,
        scratch_shapes=[
            vmem((rows, model), low),
            vmem((2, 8 * rows, model), low),
            vmem((blocks, n * depth, 2 * LANES), low),
            vmem((n, cuts, part, sub), low),
            vmem((8 * rows, part), low),
            vmem((8 * rows, part), low),
            vmem((2, 4 * rows, sub), full),
            vmem((n * cuts, 4 * rows, sub), low),
            vmem((n * cuts, 4 * rows, sub), low),
            vmem((n * cuts, 2, rows, sub // 2), low),
            vmem((n * cuts, 2, rows, sub // 2), low),
            vmem((n * cuts, 2, rows, sub), low),
            vmem((n * cuts, 2, rows, sub), low),
            vmem((n * cuts, rows, sub), full),
            vmem((rows, sub // 2), full),
            dma(()),
            dma((blocks, 2)),
            dma((cuts,)),
            dma((4,)),
            dma((4,)),
            dma((2, 20)),
            dma((2, 20)),
            dma((2, blocks)),
            dma((n, blocks)),
            dma((2, n, cuts)),
            dma((n, cuts)),
            dma((blocks, 4)),
            dma((blocks, 4)),
            dma((n * cuts,)),
            dma((n * cuts,)),
            dma((n * cuts, 2)),
            dma((n * cuts, 2)),
            dma((n * cuts, 2)),
            dma((n * cuts, 2)),
        ],
        compiler_params=pltpu.CompilerParams(
            collective_id=0, has_side_effects=True, vmem_limit_bytes=56 * 2**20
        ),
    )(tokens, norm_gain.reshape(1, -1), w_gate, w_up, w_down, post_gain.reshape(1, -1))


def solution(mesh):
    n = mesh.shape["fs"]

    def body(tokens, norm_gain, w_gate, w_up, w_down, post_gain):
        args = (tokens, norm_gain, w_gate, w_up, w_down, post_gain)
        rows = tokens.shape[0]
        fits = (
            mesh.shape["rep"] == 2 and mesh.shape["tp"] == 4 and n == 4 and rows <= 128
            and w_gate.shape[1] == 6 * LANES and w_down.shape[1] == 2 * PIECE
            and rows % 64 == 0 and w_gate.shape[1] % 256 == 0 and w_down.shape[1] % PIECE == 0
        )
        return chain_body(n, *args) if fits else plain_body(*args)

    return jax.shard_map(
        body,
        mesh=mesh,
        in_specs=(
            P(("rep", "fs", "tp"), None),
            P(),
            P("fs", "tp"),
            P("fs", "tp"),
            P("tp", "fs"),
            P(),
        ),
        out_specs=P(("rep", "fs", "tp"), None),
        check_vma=False,
    )
```

time: 94.1 us -> 79.8 us (0.85)
  Pallas kernels: 92 us -> 78.7 us
  local copies, waits for them, and re-layouts: 1.88 us -> 0.8 us
    pallas_call x1, Pallas kernels: 92 us -> 78.7 us  [chain_body(): pl.pallas_call(functools.partial(kernel, n, rows, depth, part, width, cut...]
    unnamed x1, local copies, waits for them, and re-layouts: 1.88 us -> 0.8 us
where the time goes in v2:
time: 79.8 us; the launch traced here: 79.5 us
  Pallas kernels  78.7 us (99%)
  local copies, waits for them, and re-layouts  0.8 us (1%)
    pallas_call x1, Pallas kernels, chain_body(): pl.pallas_call(functools.partial(kernel, n, rows, depth, part, width, cut...  78.7 us

profile of v2, /device:TPU:0, one launch (start us, length us, event | category | flops | bytes accessed | tf_op | source)
XLA Modules:
  0.0 79.5 jit_solution(11571144614569670700)
XLA Ops:
  0.0 78.7 %shard_map.64 = bf16[128,2048]{1,0:T(8,128)(2,1)S(1)} custom-call(bf16[128,2048]{1,0:T(8,128)(2,1)} %tok_ref.1, f32[1,2048]{1,0:T(1,128)} %bitcast.2, bf16[512,768]{1,0:T(8,128)(2,1)} %wg_ref.1, bf16[512,768]{1,0:T(8,128)(2,1)} %wu_ref.1, bf16[768,512]{1,0:T(8,128)(2,1)} %wd_ref.1, f32[1,2048]{1,0:T(1,128)} %bitcast.3), custom_call_target="tpu_custom_call" | custom-call | tf_op jit(solution)/shard_map/pallas_call | solution.py:440
  78.7 0.8 %copy.8 = bf16[128,2048]{1,0:T(8,128)(2,1)} copy(bf16[128,2048]{1,0:T(8,128)(2,1)S(1)} %shard_map.64) | data formatting | bytes 1048576

commit v3 on v2

v3 whole, which is shorter than its diff:
```python
import functools

import jax
import jax.numpy as jnp
from jax import lax
from jax.experimental import pallas as pl
from jax.experimental.pallas import tpu as pltpu
from jax.sharding import PartitionSpec as P

EPS = 1e-06
MESH = pl.DeviceIdType.MESH
PIECE = 256
LANES = 128


def rms_scale(values, gain):
    return values * lax.rsqrt(jnp.mean(values * values, axis=-1, keepdims=True) + EPS) * gain


def plain_body(tokens, norm_gain, w_gate, w_up, w_down, post_gain):
    own_normed = rms_scale(tokens.astype(jnp.float32), norm_gain).astype(jnp.bfloat16)
    normed = lax.all_gather(own_normed, "tp", axis=0, tiled=True)
    gate = jnp.dot(
        normed, lax.all_gather(w_gate, "fs", axis=0, tiled=True), preferred_element_type=jnp.float32
    )
    up = jnp.dot(
        normed, lax.all_gather(w_up, "fs", axis=0, tiled=True), preferred_element_type=jnp.float32
    )
    hidden = (jax.nn.silu(gate) * up).astype(jnp.bfloat16)
    terms = jnp.dot(
        hidden, lax.all_gather(w_down, "fs", axis=1, tiled=True), preferred_element_type=jnp.float32
    )
    summed = lax.psum_scatter(
        terms.astype(jnp.bfloat16), "tp", scatter_dimension=0, tiled=True
    ).astype(jnp.float32)
    return rms_scale(summed, post_gain).astype(jnp.bfloat16)


def kernel(
    n, rows, depth, part, width, cuts, lanes,
    tok_ref, gain_ref, wg_ref, wu_ref, wd_ref, post_ref, out_ref,
    raw, tok, gu, dn, hid, hdel, kept, pair_out, pair_in, half_out, half_in, full_out, full_in, fin, squares,
    tok_l, gu_l, dn_l, z_s, z_r, tok_s, tok_r, gu_s, gu_r, dn_s, dn_r, hid_s, hid_r,
    pair_s, pair_r, half_s, half_r, full_s, full_r,
):
    r, k, t = lax.axis_index("rep"), lax.axis_index("fs"), lax.axis_index("tp")
    x, c = t // 2, t % 2
    t_pair, t_x, r_y = x * 2 + (1 - c), (1 - x) * 2 + c, 1 - r
    t_px = (1 - x) * 2 + (1 - c)
    partner, along_x, along_y, diag = {"tp": t_pair}, {"tp": t_x}, {"rep": r_y}, {"rep": r_y, "tp": t_x}
    left = k < n // 2
    last = jnp.where(left, 0, n - 1)
    near = jnp.where(left, 1, n - 2)
    far_near, far_last = n - 1 - near, n - 1 - last
    at_end = k == last
    in_middle = k != last
    inner, outer = {"fs": jnp.where(left, k + 1, k - 1)}, {"fs": last}
    blocks = part // lanes
    sub = width // cuts
    half = pl.multiple_of(r * part, part)
    piece = rows // 4
    own_depth = pl.ds(pl.multiple_of(k * depth, depth), depth)

    def gu_load(b, q):
        ref = (wg_ref, wu_ref)[q]
        return pltpu.make_async_copy(
            ref.at[:, pl.ds(half + b * lanes, lanes)], gu.at[b, own_depth, pl.ds(q * lanes, lanes)], gu_l.at[b]
        )

    def dn_load(j):
        return pltpu.make_async_copy(wd_ref.at[pl.ds(half, part), pl.ds(j * sub, sub)], dn.at[k, j], dn_l)

    tok_load = pltpu.make_async_copy(tok_ref, raw, tok_l)

    tok_load.start()
    for b in range(blocks):
        for q in (0, 1):
            gu_load(b, q).start()
    for j in range(cuts):
        dn_load(j).start()

    barrier = pltpu.get_barrier_semaphore()
    for where in (partner, along_x, along_y, diag, inner):
        pl.semaphore_signal(barrier, inc=1, device_id=where, device_id_type=MESH)

    @pl.when(in_middle)
    def _():
        pl.semaphore_signal(barrier, inc=1, device_id=outer, device_id_type=MESH)

    pl.semaphore_wait(barrier, 5 + jnp.where(in_middle, 1, 0))

    def remote(ref, send, recv, where, to=None):
        return pltpu.make_async_remote_copy(
            ref, ref if to is None else to, send, recv, device_id=where, device_id_type=MESH
        )

    def gu_at(s, b):
        return gu.at[b, pl.ds(pl.multiple_of(s * depth, depth), depth)]

    def gu_send(kind, b):
        return remote(
            gu_at(last if kind else k, b), gu_s.at[kind], gu_r.at[b + jnp.where(in_middle, blocks, 0)], inner
        )

    def gu_pass(b):
        remote(gu_at(last, b), gu_s.at[1], gu_r.at[b], inner).wait_recv()
        gu_send(1, b).start()

    def gu_wait(b):
        remote(gu.at[b, pl.ds(0, 2 * depth)], gu_s.at[0], gu_r.at[blocks + b], inner).wait_recv()

    def dn_send(way, s, j):
        return remote(dn.at[s, j], dn_s.at[way], dn_r.at[s, j], outer if way else inner)

    def dn_wait(s, j):
        remote(dn.at[s, j], dn_s.at[0], dn_r.at[s, j], inner).wait_recv()

    def pass_down(way, s, j):
        dn_wait(s, j)
        dn_send(way, s, j).start()

    def rows_of(p, r_at, t_at, first, count):
        base = (r_at * 4 + (t_at % 2) * 2 + t_at // 2) * rows
        return tok.at[p, pl.ds(base + first * piece, count * piece)]

    def z_send(i):
        return remote(rows_of(0, r, t, i, 1), z_s, z_r.at[i], inner, rows_of(1, r, t, i, 1))

    def z_wait(i):
        remote(rows_of(1, r, t, i, 1), z_s, z_r.at[i], inner).wait_recv()

    sends = (
        [((r, t, i, 1), along_x) for i in range(4)]
        + [((r, t, i, 1), along_y) for i in range(4)]
        + [((r, t_x, 0, 1), along_y), ((r, t_x, 1, 1), along_y), ((r_y, t, 2, 1), along_x), ((r_y, t, 3, 1), along_x)]
        + [((r_at, t_at, i, 2), partner) for r_at, t_at in ((r, t), (r, t_x), (r_y, t), (r_y, t_x)) for i in (0, 2)]
    )
    groups = (
        ((0, 1), (6, 7), (2, 3), (4, 5), (8, 9), (10, 11), (12, 13, 14, 15), (16, 17, 18, 19)),
        ((0, 4), (1, 5), (6,), (7,), (2, 3), (8, 9), (10, 11), (12, 13, 14, 15, 16, 17, 18, 19)),
    )

    def group_of(p, i):
        return [g for g, held in enumerate(groups[p]) if i in held][0]

    def go(p, *which):
        for i in which:
            at, where = sends[i]
            remote(rows_of(p, *at), tok_s.at[p], tok_r.at[p, group_of(p, i)], where).start()

    def got(p, *which):
        g = group_of(p, which[0])
        assert groups[p][g] == which
        count = sum(1 if i < 12 else 2 for i in which) * piece
        remote(tok.at[p, pl.ds(0, count)], tok_s.at[p], tok_r.at[p, g], partner).wait_recv()

    quarter = 2 * rows
    halves = 4 * rows

    def half_rows(r_at):
        return pl.ds(pl.multiple_of(r_at * halves, halves), halves)

    def hid_send(b, r_at):
        at = (half_rows(r_at), pl.ds(b * lanes, lanes))
        return remote(hdel.at[at], hid_s, hid_r.at[r_at], outer, hid.at[at])

    def hid_wait(r_at):
        remote(hid.at[half_rows(r_at)], hid_s, hid_r.at[r_at], partner).wait_recv()

    def gated(p, b, r_at):
        at = half_rows(r_at)
        both = jnp.dot(tok[p, at, :], gu[b], preferred_element_type=jnp.float32)
        gate, up = both[:, :lanes], both[:, lanes:]
        value = (gate / (1.0 + jnp.exp(-gate)) * up).astype(jnp.bfloat16)
        (hdel if p else hid)[at, pl.ds(b * lanes, lanes)] = value

    def passed_block(b):
        @pl.loop(0, 2)
        def _(i):
            r_at = (r_y + i) % 2
            gated(1, b, r_at)
            hid_send(b, r_at).start()

    def own_block(b, r_at):
        gated(0, b, r_at)

    def send_own_gu():
        for b in range(blocks):
            pltpu.make_async_copy(gu.at[b, own_depth], gu.at[b, own_depth], gu_l.at[b]).wait()
            gu_send(0, b).start()

    def send_own_dn(way):
        pltpu.make_async_copy(dn.at[k], dn.at[k], dn_l).wait()
        for j in range(cuts):
            dn_send(way, k, j).start()

    @pl.when(in_middle)
    def _():
        send_own_gu()
        send_own_dn(1)

    tok_load.wait()
    tile = 32
    first = (r * 4 + c * 2 + x) * rows

    @pl.loop(0, rows // tile)
    def _(i):
        at = pl.ds(pl.multiple_of(i * tile, tile), tile)
        to = pl.ds(pl.multiple_of(first + i * tile, tile), tile)
        tok[0, to, :] = rms_scale(raw[at, :].astype(jnp.float32), gain_ref[...]).astype(jnp.bfloat16)

    @pl.when(at_end)
    def _():
        for i in range(4):
            z_send(i).start()
        send_own_gu()
        send_own_dn(0)

    @pl.when(in_middle)
    def _():
        go(0, 0, 1, 6, 7, 12, 13)
        z_wait(0)
        go(1, 0, 4)
        got(0, 0, 1)
        go(0, 14)
        got(0, 6, 7)
        go(0, 17)
        z_wait(1)
        go(1, 1, 5, 12)
        got(1, 0, 4)
        z_wait(2)
        go(1, 2, 6)
        got(1, 1, 5)
        go(1, 14, 16)
        z_wait(3)
        go(1, 13, 3, 7, 8, 9)
        got(1, 6)
        go(1, 10)
        got(1, 7)
        go(1, 17, 11)
        got(1, 2, 3)
        go(1, 15)
        gu_pass(0)
        go(0, 2, 4)
        gu_pass(1)
        got(1, 8, 9)
        go(1, 18)
        got(1, 10, 11)
        go(1, 19)
        go(0, 3, 5, 8, 10)
        got(1, 12, 13, 14, 15, 16, 17, 18, 19)
        gu_wait(0)
        passed_block(0)
        go(0, 9, 11)
        got(0, 2, 3)
        go(0, 15)
        got(0, 4, 5)
        go(0, 16)
        gu_pass(2)
        gu_wait(1)
        passed_block(1)
        got(0, 12, 13, 14, 15)
        own_block(0, r)
        own_block(1, r)
        dn_wait(last, 0)
        got(0, 8, 9)
        go(0, 18)
        got(0, 10, 11)
        go(0, 19)
        gu_wait(2)
        for j in range(cuts):
            dn_send(0, k, j).start()
        dn_send(0, last, 0).start()
        passed_block(2)
        own_block(2, r)
        pass_down(0, last, 1)
        got(0, 16, 17, 18, 19)
        own_block(0, r_y)
        own_block(1, r_y)
        own_block(2, r_y)
        pass_down(1, far_near, 0)

    chunks = n * cuts
    mid = sub // 2
    here, there = 0, 1

    def pair_copy(p, side):
        return remote(pair_out.at[p, side], pair_s, pair_r.at[p, side], partner, pair_in.at[p, side])

    def half_copy(p, way):
        return remote(
            half_out.at[p, way], half_s, half_r.at[p], along_y if way else along_x, half_in.at[p, way]
        )

    def full_copy(p, way):
        return remote(
            full_out.at[p, way], full_s, full_r.at[p], along_y if way else along_x, full_in.at[p, way]
        )

    def source(i):
        near_or_last = jnp.where(i == 0, k, near + last - k)
        return jnp.where(i < 2, near_or_last, jnp.where(i == 2, far_near, far_last))

    def place(at):
        return source(at // cuts) * cuts + at % cuts

    def product(at, side):
        s, j, p = source(at // cuts), at % cuts, place(at)
        r_at = r_y if side == there else r
        first = pl.multiple_of(r_at * halves, halves)

        def part_of(core):
            rows_at = pl.ds(pl.multiple_of(first + core * quarter, quarter), quarter)
            return jnp.dot(hid[rows_at, :], dn[s, j], preferred_element_type=jnp.float32)

        pair_out[p, side] = part_of(1 - c).astype(jnp.bfloat16)
        pair_copy(p, side).start()
        kept[p, side] = part_of(c)

    def of(m):
        return pl.ds(pl.multiple_of(m * rows, rows), rows)

    def summed(p, side, x_at):
        return kept[p, side, of(x_at), :] + pair_in[p, side, of(x_at), :].astype(jnp.float32)

    def finish_there(at):
        p = place(at)
        pair_copy(p, there).wait_recv()
        across = summed(p, there, 1 - x).astype(jnp.bfloat16)
        half_out[p, 0] = across[:, :mid]
        half_out[p, 1] = across[:, mid:]
        half_copy(p, 0).start()
        half_copy(p, 1).start()
        kept[p, there, of(x), :] = summed(p, there, x)

    def finish_here(at):
        p = place(at)
        pair_copy(p, here).wait_recv()
        kept[p, here, of(1 - x), :] = summed(p, here, 1 - x)
        fin[p] = summed(p, here, x)

    def finish_half(at):
        p = place(at)
        remote(half_in.at[p], half_s, half_r.at[p], partner).wait_recv()
        to_x, to_y = (here, of(1 - x)), (there, of(x))
        full_out[p, 0, :, :mid] = kept[(p, *to_x, slice(0, mid))].astype(jnp.bfloat16)
        full_out[p, 0, :, mid:] = (kept[(p, *to_x, slice(mid, sub))] + half_in[p, 1].astype(jnp.float32)).astype(jnp.bfloat16)
        full_copy(p, 0).start()
        full_out[p, 1, :, mid:] = kept[(p, *to_y, slice(mid, sub))].astype(jnp.bfloat16)
        full_out[p, 1, :, :mid] = (kept[(p, *to_y, slice(0, mid))] + half_in[p, 0].astype(jnp.float32)).astype(jnp.bfloat16)
        full_copy(p, 1).start()

    early = 2 * cuts

    @pl.when(at_end)
    def _():
        for j in range(cuts):
            dn_wait(near, j)
        hid_wait(r_y)

    @pl.loop(0, early)
    def _(at):
        product(at, there)

        @pl.when(at > 0)
        def _():
            finish_there(at - 1)

    @pl.when(at_end)
    def _():
        hid_wait(r)

    @pl.when(in_middle)
    def _():
        pass_down(1, far_near, 1)

    @pl.loop(0, early)
    def _(at):
        product(at, here)

        @pl.when(at == 0)
        def _():
            finish_there(early - 1)

        @pl.when(at > 0)
        def _():
            finish_here(at - 1)
            finish_half(at - 1)

        @pl.when(in_middle & (at == 2))
        def _():
            pass_down(1, far_last, 0)

    @pl.loop(early, chunks)
    def _(at):
        @pl.when(at_end)
        def _():
            dn_wait(source(at // cuts), at % cuts)

        @pl.when(in_middle & (at == early))
        def _():
            pass_down(1, far_last, 1)

        product(at, there)
        product(at, here)

        @pl.when(at == early)
        def _():
            finish_here(at - 1)
            finish_half(at - 1)

        finish_there(at)
        finish_here(at)

        @pl.when(at > early)
        def _():
            finish_half(at - 1)

    finish_half(chunks - 1)

    remote(gu.at[:, pl.ds(0, depth)], gu_s.at[0], gu_r.at[0], inner).wait_send()

    @pl.when(at_end)
    def _():
        remote(tok.at[0, pl.ds(0, rows)], z_s, z_r.at[0], inner).wait_send()
        remote(dn.at[0], dn_s.at[0], dn_r.at[0, 0], inner).wait_send()

    @pl.when(in_middle)
    def _():
        for p in (0, 1):
            total = sum(1 if i < 12 else 2 for i in range(len(sends))) * piece
            remote(tok.at[p, pl.ds(0, total)], tok_s.at[p], tok_r.at[p, 0], partner).wait_send()
        remote(gu.at[:, pl.ds(0, depth)], gu_s.at[1], gu_r.at[0], inner).wait_send()
        remote(hdel, hid_s, hid_r.at[0], outer).wait_send()
        remote(dn.at[pl.ds(0, 2)], dn_s.at[0], dn_r.at[0, 0], inner).wait_send()
        remote(dn.at[pl.ds(0, 3)], dn_s.at[1], dn_r.at[0, 0], outer).wait_send()

    remote(pair_out, pair_s, pair_r.at[0, 0], partner).wait_send()
    remote(half_out, half_s, half_r.at[0], along_x).wait_send()

    squares[...] = jnp.zeros_like(squares)

    @pl.loop(0, chunks)
    def _(at):
        p = place(at)
        remote(full_in.at[p], full_s, full_r.at[p], along_x).wait_recv()
        total = fin[p] + full_in[p, 0].astype(jnp.float32) + full_in[p, 1].astype(jnp.float32)
        fin[p] = total
        squares[...] += total[:, :mid] * total[:, :mid] + total[:, mid:] * total[:, mid:]

    scale = lax.rsqrt(jnp.sum(squares[...], axis=-1, keepdims=True) / (n * width) + EPS)
    for p in range(chunks):
        cols = pl.ds(p * sub, sub)
        out_ref[:, cols] = (fin[p] * scale * post_ref[:, cols]).astype(out_ref.dtype)

    remote(full_out, full_s, full_r.at[0], along_x).wait_send()


def chain_body(n, tokens, norm_gain, w_gate, w_up, w_down, post_gain):
    rows, model = tokens.shape
    depth, block = w_gate.shape
    width = w_down.shape[1]
    part = block // 2
    cuts = width // PIECE
    sub = width // cuts
    blocks = part // LANES
    chunks = n * cuts
    vmem, dma = pltpu.VMEM, pltpu.SemaphoreType.DMA
    low, full = jnp.bfloat16, jnp.float32
    anywhere = pl.BlockSpec(memory_space=pl.ANY)
    inside = pl.BlockSpec(memory_space=vmem)
    return pl.pallas_call(
        functools.partial(kernel, n, rows, depth, part, width, cuts, LANES),
        out_shape=pltpu.VMEM((rows, model), low),
        in_specs=[anywhere, inside, anywhere, anywhere, anywhere, inside],
        out_specs=inside,
        scratch_shapes=[
            vmem((rows, model), low),
            vmem((2, 8 * rows, model), low),
            vmem((blocks, n * depth, 2 * LANES), low),
            vmem((n, cuts, part, sub), low),
            vmem((8 * rows, part), low),
            vmem((8 * rows, part), low),
            vmem((chunks, 2, 2 * rows, sub), full),
            vmem((chunks, 2, 2 * rows, sub), low),
            vmem((chunks, 2, 2 * rows, sub), low),
            vmem((chunks, 2, rows, sub // 2), low),
            vmem((chunks, 2, rows, sub // 2), low),
            vmem((chunks, 2, rows, sub), low),
            vmem((chunks, 2, rows, sub), low),
            vmem((chunks, rows, sub), full),
            vmem((rows, sub // 2), full),
            dma(()),
            dma((blocks,)),
            dma(()),
            dma(()),
            dma((4,)),
            dma((2,)),
            dma((2, 8)),
            dma((2,)),
            dma((2 * blocks,)),
            dma((2,)),
            dma((n, cuts)),
            dma(()),
            dma((2,)),
            dma(()),
            dma((chunks, 2)),
            dma(()),
            dma((chunks,)),
            dma(()),
            dma((chunks,)),
        ],
        compiler_params=pltpu.CompilerParams(
            collective_id=0, has_side_effects=True, vmem_limit_bytes=56 * 2**20
        ),
    )(tokens, norm_gain.reshape(1, -1), w_gate, w_up, w_down, post_gain.reshape(1, -1))


def solution(mesh):
    n = mesh.shape["fs"]

    def body(tokens, norm_gain, w_gate, w_up, w_down, post_gain):
        args = (tokens, norm_gain, w_gate, w_up, w_down, post_gain)
        rows = tokens.shape[0]
        fits = (
            mesh.shape["rep"] == 2 and mesh.shape["tp"] == 4 and n == 4 and rows <= 128 and rows % 128 == 0
            and w_gate.shape[1] == 6 * LANES and w_down.shape[1] == 2 * PIECE
        )
        return chain_body(n, *args) if fits else plain_body(*args)

    return jax.shard_map(
        body,
        mesh=mesh,
        in_specs=(
            P(("rep", "fs", "tp"), None),
            P(),
            P("fs", "tp"),
            P("fs", "tp"),
            P("tp", "fs"),
            P(),
        ),
        out_specs=P(("rep", "fs", "tp"), None),
        check_vma=False,
    )
```

time: 79.8 us -> 78.3 us (0.981)
  Pallas kernels: 78.7 us -> 77.3 us
    pallas_call x1, Pallas kernels: 78.7 us -> 77.3 us  [chain_body(): pl.pallas_call(functools.partial(kernel, n, rows, depth, part, width, cut...]
where the time goes in v3:
time: 78.3 us; the launch traced here: 78.1 us
  Pallas kernels  77.3 us (99%)
  local copies, waits for them, and re-layouts  0.8 us (1%)
    pallas_call x1, Pallas kernels, chain_body(): pl.pallas_call(functools.partial(kernel, n, rows, depth, part, width, cut...  77.3 us

profile of v3, /device:TPU:0, one launch (start us, length us, event | category | flops | bytes accessed | tf_op | source)
XLA Modules:
  0.0 78.1 jit_solution(15031945190923694933)
XLA Ops:
  0.0 77.3 %shard_map.64 = bf16[128,2048]{1,0:T(8,128)(2,1)S(1)} custom-call(bf16[128,2048]{1,0:T(8,128)(2,1)} %tok_ref.1, f32[1,2048]{1,0:T(1,128)} %bitcast.2, bf16[512,768]{1,0:T(8,128)(2,1)} %wg_ref.1, bf16[512,768]{1,0:T(8,128)(2,1)} %wu_ref.1, bf16[768,512]{1,0:T(8,128)(2,1)} %wd_ref.1, f32[1,2048]{1,0:T(1,128)} %bitcast.3), custom_call_target="tpu_custom_call" | custom-call | tf_op jit(solution)/shard_map/pallas_call | solution.py:472
  77.3 0.8 %copy.8 = bf16[128,2048]{1,0:T(8,128)(2,1)} copy(bf16[128,2048]{1,0:T(8,128)(2,1)S(1)} %shard_map.64) | data formatting | bytes 1048576

commit v4 on v3

--- a/solution.py
+++ b/solution.py
@@ -39,9 +39,9 @@
 def kernel(
     n, rows, depth, part, width, cuts, lanes,
     tok_ref, gain_ref, wg_ref, wu_ref, wd_ref, post_ref, out_ref,
-    raw, tok, gu, dn, hid, hdel, kept, pair_out, pair_in, half_out, half_in, full_out, full_in, fin, squares,
+    raw, tok, gu, dn, hid, kept, pair_out, pair_in, half_out, half_in, full_out, full_in, fin, res_out, res_in, squares,
     tok_l, gu_l, dn_l, z_s, z_r, tok_s, tok_r, gu_s, gu_r, dn_s, dn_r, hid_s, hid_r,
-    pair_s, pair_r, half_s, half_r, full_s, full_r,
+    pair_s, pair_r, half_s, half_r, full_s, full_r, res_s, res_r,
 ):
     r, k, t = lax.axis_index("rep"), lax.axis_index("fs"), lax.axis_index("tp")
     x, c = t // 2, t % 2
@@ -68,7 +68,7 @@
         )
 
     def dn_load(j):
-        return pltpu.make_async_copy(wd_ref.at[pl.ds(half, part), pl.ds(j * sub, sub)], dn.at[k, j], dn_l)
+        return pltpu.make_async_copy(wd_ref.at[pl.ds(half, part), pl.ds(j * sub, sub)], dn.at[k * cuts + j], dn_l)
 
     tok_load = pltpu.make_async_copy(tok_ref, raw, tok_l)
 
@@ -110,24 +110,27 @@
         remote(gu.at[b, pl.ds(0, 2 * depth)], gu_s.at[0], gu_r.at[blocks + b], inner).wait_recv()
 
     def dn_send(way, s, j):
-        return remote(dn.at[s, j], dn_s.at[way], dn_r.at[s, j], outer if way else inner)
+        at = s * cuts + j
+        return remote(dn.at[at], dn_s.at[way], dn_r.at[at], outer if way else inner)
 
     def dn_wait(s, j):
-        remote(dn.at[s, j], dn_s.at[0], dn_r.at[s, j], inner).wait_recv()
+        at = s * cuts + j
+        remote(dn.at[at], dn_s.at[0], dn_r.at[at], inner).wait_recv()
 
     def pass_down(way, s, j):
         dn_wait(s, j)
         dn_send(way, s, j).start()
 
-    def rows_of(p, r_at, t_at, first, count):
-        base = (r_at * 4 + (t_at % 2) * 2 + t_at // 2) * rows
+    def rows_of(p, r_at, t_at, first, count, core):
+        other = (t_at % 2 + core) % 2
+        base = (r_at * 4 + other * 2 + t_at // 2) * rows
         return tok.at[p, pl.ds(base + first * piece, count * piece)]
 
     def z_send(i):
-        return remote(rows_of(0, r, t, i, 1), z_s, z_r.at[i], inner, rows_of(1, r, t, i, 1))
+        return remote(rows_of(0, r, t, i, 1, c), z_s, z_r.at[i], inner, rows_of(1, r, t, i, 1, c))
 
     def z_wait(i):
-        remote(rows_of(1, r, t, i, 1), z_s, z_r.at[i], inner).wait_recv()
+        remote(rows_of(1, r, t, i, 1, c), z_s, z_r.at[i], inner).wait_recv()
 
     sends = (
         [((r, t, i, 1), along_x) for i in range(4)]
@@ -146,7 +149,8 @@
     def go(p, *which):
         for i in which:
             at, where = sends[i]
-            remote(rows_of(p, *at), tok_s.at[p], tok_r.at[p, group_of(p, i)], where).start()
+            to = rows_of(p, *at, 1 - c if i >= 12 else c)
+            remote(rows_of(p, *at, c), tok_s.at[p], tok_r.at[p, group_of(p, i)], where, to).start()
 
     def got(p, *which):
         g = group_of(p, which[0])
@@ -160,29 +164,19 @@
     def half_rows(r_at):
         return pl.ds(pl.multiple_of(r_at * halves, halves), halves)
 
+    def hid_at(p, b, r_at):
+        return hid.at[p, half_rows(r_at), pl.ds(pl.multiple_of(b * lanes, lanes), lanes)]
+
     def hid_send(b, r_at):
-        at = (half_rows(r_at), pl.ds(b * lanes, lanes))
-        return remote(hdel.at[at], hid_s, hid_r.at[r_at], outer, hid.at[at])
+        return remote(hid_at(1, b, r_at), hid_s, hid_r.at[r_at], outer, hid_at(0, b, r_at))
 
     def hid_wait(r_at):
-        remote(hid.at[half_rows(r_at)], hid_s, hid_r.at[r_at], partner).wait_recv()
+        remote(hid.at[0, half_rows(r_at)], hid_s, hid_r.at[r_at], partner).wait_recv()
 
     def gated(p, b, r_at):
-        at = half_rows(r_at)
-        both = jnp.dot(tok[p, at, :], gu[b], preferred_element_type=jnp.float32)
+        both = jnp.dot(tok[p, half_rows(r_at), :], gu[b], preferred_element_type=jnp.float32)
         gate, up = both[:, :lanes], both[:, lanes:]
-        value = (gate / (1.0 + jnp.exp(-gate)) * up).astype(jnp.bfloat16)
-        (hdel if p else hid)[at, pl.ds(b * lanes, lanes)] = value
-
-    def passed_block(b):
-        @pl.loop(0, 2)
-        def _(i):
-            r_at = (r_y + i) % 2
-            gated(1, b, r_at)
-            hid_send(b, r_at).start()
-
-    def own_block(b, r_at):
-        gated(0, b, r_at)
+        hid_at(p, b, r_at)[...] = (gate / (1.0 + jnp.exp(-gate)) * up).astype(jnp.bfloat16)
 
     def send_own_gu():
         for b in range(blocks):
@@ -190,7 +184,8 @@
             gu_send(0, b).start()
 
     def send_own_dn(way):
-        pltpu.make_async_copy(dn.at[k], dn.at[k], dn_l).wait()
+        own = dn.at[pl.ds(k * cuts, cuts)]
+        pltpu.make_async_copy(own, own, dn_l).wait()
         for j in range(cuts):
             dn_send(way, k, j).start()
 
@@ -201,7 +196,7 @@
 
     tok_load.wait()
     tile = 32
-    first = (r * 4 + c * 2 + x) * rows
+    first = (r * 4 + x) * rows
 
     @pl.loop(0, rows // tile)
     def _(i):
@@ -218,66 +213,86 @@
 
     @pl.when(in_middle)
     def _():
-        go(0, 0, 1, 6, 7, 12, 13)
-        z_wait(0)
-        go(1, 0, 4)
-        got(0, 0, 1)
-        go(0, 14)
-        got(0, 6, 7)
-        go(0, 17)
-        z_wait(1)
-        go(1, 1, 5, 12)
-        got(1, 0, 4)
-        z_wait(2)
-        go(1, 2, 6)
-        got(1, 1, 5)
-        go(1, 14, 16)
-        z_wait(3)
-        go(1, 13, 3, 7, 8, 9)
-        got(1, 6)
-        go(1, 10)
-        got(1, 7)
-        go(1, 17, 11)
-        got(1, 2, 3)
-        go(1, 15)
-        gu_pass(0)
-        go(0, 2, 4)
-        gu_pass(1)
-        got(1, 8, 9)
-        go(1, 18)
-        got(1, 10, 11)
-        go(1, 19)
-        go(0, 3, 5, 8, 10)
-        got(1, 12, 13, 14, 15, 16, 17, 18, 19)
-        gu_wait(0)
-        passed_block(0)
-        go(0, 9, 11)
-        got(0, 2, 3)
-        go(0, 15)
-        got(0, 4, 5)
-        go(0, 16)
-        gu_pass(2)
-        gu_wait(1)
-        passed_block(1)
-        got(0, 12, 13, 14, 15)
-        own_block(0, r)
-        own_block(1, r)
-        dn_wait(last, 0)
-        got(0, 8, 9)
-        go(0, 18)
-        got(0, 10, 11)
-        go(0, 19)
-        gu_wait(2)
-        for j in range(cuts):
-            dn_send(0, k, j).start()
-        dn_send(0, last, 0).start()
-        passed_block(2)
-        own_block(2, r)
-        pass_down(0, last, 1)
-        got(0, 16, 17, 18, 19)
-        own_block(0, r_y)
-        own_block(1, r_y)
-        own_block(2, r_y)
+        @pl.loop(0, 12)
+        def _(at_step):
+            def step(at):
+                return pl.when(at_step == at)
+
+            @step(0)
+            def _():
+                go(0, 0, 1, 6, 7, 12, 13)
+                z_wait(0)
+                go(1, 0, 4)
+                got(0, 0, 1)
+                go(0, 14)
+                got(0, 6, 7)
+                go(0, 17)
+                z_wait(1)
+                go(1, 1, 5, 12)
+                got(1, 0, 4)
+                z_wait(2)
+                go(1, 2, 6)
+                got(1, 1, 5)
+                go(1, 14, 16)
+                z_wait(3)
+                go(1, 13, 3, 7, 8, 9)
+                got(1, 6)
+                go(1, 10)
+                got(1, 7)
+                go(1, 17, 11)
+                got(1, 2, 3)
+                go(1, 15)
+                gu_pass(0)
+                go(0, 2, 4)
+                gu_pass(1)
+                got(1, 8, 9)
+                go(1, 18)
+                got(1, 10, 11)
+                go(1, 19)
+                go(0, 3, 5, 8, 10)
+                got(1, 12, 13, 14, 15, 16, 17, 18, 19)
+                gu_wait(0)
+
+            @step(2)
+            def _():
+                go(0, 9, 11)
+                got(0, 2, 3)
+                go(0, 15)
+                got(0, 4, 5)
+                go(0, 16)
+                gu_pass(2)
+                gu_wait(1)
+
+            @step(4)
+            def _():
+                got(0, 12, 13, 14, 15)
+
+            @step(6)
+            def _():
+                dn_wait(last, 0)
+                got(0, 8, 9)
+                go(0, 18)
+                got(0, 10, 11)
+                go(0, 19)
+                gu_wait(2)
+                for j in range(cuts):
+                    dn_send(0, k, j).start()
+                dn_send(0, last, 0).start()
+
+            @step(9)
+            def _():
+                pass_down(0, last, 1)
+                got(0, 16, 17, 18, 19)
+
+            passed = (at_step < 4) | (at_step == 6) | (at_step == 7)
+            b = jnp.where(at_step < 4, at_step // 2, jnp.where(at_step < 6, at_step - 4, jnp.where(at_step < 9, 2, at_step - 9)))
+            r_at = jnp.where(passed, (r_y + at_step % 2) % 2, jnp.where(at_step < 9, r, r_y))
+            gated(jnp.where(passed, 1, 0), b, r_at)
+
+            @pl.when(passed)
+            def _():
+                hid_send(b, r_at).start()
+
         pass_down(1, far_near, 0)
 
     chunks = n * cuts
@@ -302,20 +317,16 @@
         return jnp.where(i < 2, near_or_last, jnp.where(i == 2, far_near, far_last))
 
     def place(at):
-        return source(at // cuts) * cuts + at % cuts
+        return jnp.where(at < chunks, source(at // cuts) * cuts + at % cuts, chunks)
 
     def product(at, side):
-        s, j, p = source(at // cuts), at % cuts, place(at)
-        r_at = r_y if side == there else r
-        first = pl.multiple_of(r_at * halves, halves)
-
-        def part_of(core):
-            rows_at = pl.ds(pl.multiple_of(first + core * quarter, quarter), quarter)
-            return jnp.dot(hid[rows_at, :], dn[s, j], preferred_element_type=jnp.float32)
-
-        pair_out[p, side] = part_of(1 - c).astype(jnp.bfloat16)
+        p = place(at)
+        held = jnp.where(at < chunks, p, far_last * cuts + cuts - 1)
+        rows_at = half_rows(r_y if side == there else r)
+        both = jnp.dot(hid[jnp.where(at < chunks, 0, 1), rows_at, :], dn[held], preferred_element_type=jnp.float32)
+        pair_out[p, side] = both[quarter:].astype(jnp.bfloat16)
         pair_copy(p, side).start()
-        kept[p, side] = part_of(c)
+        kept[p, side] = both[:quarter]
 
     def of(m):
         return pl.ds(pl.multiple_of(m * rows, rows), rows)
@@ -391,39 +402,52 @@
         def _():
             pass_down(1, far_last, 0)
 
-    @pl.loop(early, chunks)
-    def _(at):
-        @pl.when(at_end)
+    def order(i):
+        return jnp.where(in_middle & (i >= 2), jnp.where(i == 2, chunks, early + i - 1), early + i)
+
+    @pl.loop(0, chunks - early + 1)
+    def _(i):
+        at = order(i)
+
+        @pl.when(at_end & (i < 3))
         def _():
             dn_wait(source(at // cuts), at % cuts)
 
-        @pl.when(in_middle & (at == early))
-        def _():
-            pass_down(1, far_last, 1)
-
-        product(at, there)
-        product(at, here)
-
-        @pl.when(at == early)
-        def _():
-            finish_here(at - 1)
-            finish_half(at - 1)
-
-        finish_there(at)
-        finish_here(at)
-
-        @pl.when(at > early)
-        def _():
-            finish_half(at - 1)
-
-    finish_half(chunks - 1)
+        @pl.when(in_middle & (i == 2))
+        def _():
+            dn_wait(far_last, cuts - 1)
+
+        @pl.when(in_middle | (i < 3))
+        def _():
+            product(at, there)
+            product(at, here)
+
+        @pl.when(i == 0)
+        def _():
+            finish_here(early - 1)
+            finish_half(early - 1)
+
+        @pl.when(in_middle | (i < 3))
+        def _():
+            finish_there(at)
+            finish_here(at)
+
+        @pl.when((i > 0) & (in_middle | (i < 4)))
+        def _():
+            finish_half(order(i - 1))
+
+    @pl.when(in_middle)
+    def _():
+        finish_half(chunks - 1)
 
     remote(gu.at[:, pl.ds(0, depth)], gu_s.at[0], gu_r.at[0], inner).wait_send()
 
     @pl.when(at_end)
     def _():
         remote(tok.at[0, pl.ds(0, rows)], z_s, z_r.at[0], inner).wait_send()
-        remote(dn.at[0], dn_s.at[0], dn_r.at[0, 0], inner).wait_send()
+        remote(dn.at[pl.ds(0, cuts)], dn_s.at[0], dn_r.at[0], inner).wait_send()
+        remote(pair_out.at[pl.ds(0, chunks - 1)], pair_s, pair_r.at[0, 0], partner).wait_send()
+        remote(half_out.at[pl.ds(0, chunks - 1)], half_s, half_r.at[0], along_x).wait_send()
 
     @pl.when(in_middle)
     def _():
@@ -431,29 +455,54 @@
             total = sum(1 if i < 12 else 2 for i in range(len(sends))) * piece
             remote(tok.at[p, pl.ds(0, total)], tok_s.at[p], tok_r.at[p, 0], partner).wait_send()
         remote(gu.at[:, pl.ds(0, depth)], gu_s.at[1], gu_r.at[0], inner).wait_send()
-        remote(hdel, hid_s, hid_r.at[0], outer).wait_send()
-        remote(dn.at[pl.ds(0, 2)], dn_s.at[0], dn_r.at[0, 0], inner).wait_send()
-        remote(dn.at[pl.ds(0, 3)], dn_s.at[1], dn_r.at[0, 0], outer).wait_send()
-
-    remote(pair_out, pair_s, pair_r.at[0, 0], partner).wait_send()
-    remote(half_out, half_s, half_r.at[0], along_x).wait_send()
+        remote(hid.at[1], hid_s, hid_r.at[0], outer).wait_send()
+        remote(dn.at[pl.ds(0, 2 * cuts)], dn_s.at[0], dn_r.at[0], inner).wait_send()
+        remote(dn.at[pl.ds(0, 3 * cuts - 1)], dn_s.at[1], dn_r.at[0], outer).wait_send()
+        remote(pair_out, pair_s, pair_r.at[0, 0], partner).wait_send()
+        remote(half_out, half_s, half_r.at[0], along_x).wait_send()
 
     squares[...] = jnp.zeros_like(squares)
+
+    result = remote(res_out, res_s, res_r, outer, res_in)
+
+    def collect(at):
+        p = place(at)
+        remote(full_in.at[p], full_s, full_r.at[p], along_x).wait_recv()
+        return fin[p] + full_in[p, 0].astype(jnp.float32) + full_in[p, 1].astype(jnp.float32)
+
+    def settle(at, total):
+        fin[place(at)] = total
+        squares[...] += total[:, :mid] * total[:, :mid] + total[:, mid:] * total[:, mid:]
 
     @pl.loop(0, chunks)
     def _(at):
-        p = place(at)
-        remote(full_in.at[p], full_s, full_r.at[p], along_x).wait_recv()
-        total = fin[p] + full_in[p, 0].astype(jnp.float32) + full_in[p, 1].astype(jnp.float32)
-        fin[p] = total
-        squares[...] += total[:, :mid] * total[:, :mid] + total[:, mid:] * total[:, mid:]
+        @pl.when(in_middle & (at == chunks - 2))
+        def _():
+            res_out[...] = collect(chunks).astype(jnp.bfloat16)
+            result.start()
+
+        @pl.when(in_middle | (at < chunks - 1))
+        def _():
+            settle(at, collect(at))
+
+    @pl.when(at_end)
+    def _():
+        result.wait_recv()
+        settle(chunks - 1, res_in[...].astype(jnp.float32))
 
     scale = lax.rsqrt(jnp.sum(squares[...], axis=-1, keepdims=True) / (n * width) + EPS)
     for p in range(chunks):
         cols = pl.ds(p * sub, sub)
         out_ref[:, cols] = (fin[p] * scale * post_ref[:, cols]).astype(out_ref.dtype)
 
-    remote(full_out, full_s, full_r.at[0], along_x).wait_send()
+    @pl.when(at_end)
+    def _():
+        remote(full_out.at[pl.ds(0, chunks - 1)], full_s, full_r.at[0], along_x).wait_send()
+
+    @pl.when(in_middle)
+    def _():
+        remote(full_out, full_s, full_r.at[0], along_x).wait_send()
+        result.wait_send()
 
 
 def chain_body(n, tokens, norm_gain, w_gate, w_up, w_down, post_gain):
@@ -478,17 +527,18 @@
             vmem((rows, model), low),
             vmem((2, 8 * rows, model), low),
             vmem((blocks, n * depth, 2 * LANES), low),
-            vmem((n, cuts, part, sub), low),
-            vmem((8 * rows, part), low),
-            vmem((8 * rows, part), low),
-            vmem((chunks, 2, 2 * rows, sub), full),
-            vmem((chunks, 2, 2 * rows, sub), low),
-            vmem((chunks, 2, 2 * rows, sub), low),
-            vmem((chunks, 2, rows, sub // 2), low),
-            vmem((chunks, 2, rows, sub // 2), low),
-            vmem((chunks, 2, rows, sub), low),
-            vmem((chunks, 2, rows, sub), low),
-            vmem((chunks, rows, sub), full),
+            vmem((chunks, part, sub), low),
+            vmem((2, 8 * rows, part), low),
+            vmem((chunks + 1, 2, 2 * rows, sub), full),
+            vmem((chunks + 1, 2, 2 * rows, sub), low),
+            vmem((chunks + 1, 2, 2 * rows, sub), low),
+            vmem((chunks + 1, 2, rows, sub // 2), low),
+            vmem((chunks + 1, 2, rows, sub // 2), low),
+            vmem((chunks + 1, 2, rows, sub), low),
+            vmem((chunks + 1, 2, rows, sub), low),
+            vmem((chunks + 1, rows, sub), full),
+            vmem((rows, sub), low),
+            vmem((rows, sub), low),
             vmem((rows, sub // 2), full),
             dma(()),
             dma((blocks,)),
@@ -500,15 +550,17 @@
             dma((2,)),
             dma((2 * blocks,)),
             dma((2,)),
-            dma((n, cuts)),
+            dma((chunks,)),
             dma(()),
             dma((2,)),
             dma(()),
-            dma((chunks, 2)),
-            dma(()),
-            dma((chunks,)),
-            dma(()),
-            dma((chunks,)),
+            dma((chunks + 1, 2)),
+            dma(()),
+            dma((chunks + 1,)),
+            dma(()),
+            dma((chunks + 1,)),
+            dma(()),
+            dma(()),
         ],
         compiler_params=pltpu.CompilerParams(
             collective_id=0, has_side_effects=True, vmem_limit_bytes=56 * 2**20

time: 78.3 us -> 78 us (level)
  no operation moved by 1% of the time
where the time goes in v4:
time: 78 us; the launch traced here: 77.8 us
  Pallas kernels  77 us (99%)
  local copies, waits for them, and re-layouts  0.8 us (1%)
    pallas_call x1, Pallas kernels, chain_body(): pl.pallas_call(functools.partial(kernel, n, rows, depth, part, width, cut...  77 us

profile of v4, /device:TPU:0, one launch (start us, length us, event | category | flops | bytes accessed | tf_op | source)
XLA Modules:
  0.0 77.8 jit_solution(5200697573418697558)
XLA Ops:
  0.0 77.0 %shard_map.64 = bf16[128,2048]{1,0:T(8,128)(2,1)S(1)} custom-call(bf16[128,2048]{1,0:T(8,128)(2,1)} %tok_ref.1, f32[1,2048]{1,0:T(1,128)} %bitcast.2, bf16[512,768]{1,0:T(8,128)(2,1)} %wg_ref.1, bf16[512,768]{1,0:T(8,128)(2,1)} %wu_ref.1, bf16[768,512]{1,0:T(8,128)(2,1)} %wd_ref.1, f32[1,2048]{1,0:T(1,128)} %bitcast.3), custom_call_target="tpu_custom_call" | custom-call | tf_op jit(solution)/shard_map/pallas_call | solution.py:521
  77.0 0.8 %copy.8 = bf16[128,2048]{1,0:T(8,128)(2,1)} copy(bf16[128,2048]{1,0:T(8,128)(2,1)S(1)} %shard_map.64) | data formatting | bytes 1048576

commit v5 on v4

--- a/solution.py
+++ b/solution.py
@@ -87,6 +87,16 @@
     def _():
         pl.semaphore_signal(barrier, inc=1, device_id=outer, device_id_type=MESH)
 
+    tok_load.wait()
+    tile = 32
+    first = (r * 4 + x) * rows
+
+    @pl.loop(0, rows // tile)
+    def _(i):
+        at = pl.ds(pl.multiple_of(i * tile, tile), tile)
+        to = pl.ds(pl.multiple_of(first + i * tile, tile), tile)
+        tok[0, to, :] = rms_scale(raw[at, :].astype(jnp.float32), gain_ref[...]).astype(jnp.bfloat16)
+
     pl.semaphore_wait(barrier, 5 + jnp.where(in_middle, 1, 0))
 
     def remote(ref, send, recv, where, to=None):
@@ -193,16 +203,6 @@
     def _():
         send_own_gu()
         send_own_dn(1)
-
-    tok_load.wait()
-    tile = 32
-    first = (r * 4 + x) * rows
-
-    @pl.loop(0, rows // tile)
-    def _(i):
-        at = pl.ds(pl.multiple_of(i * tile, tile), tile)
-        to = pl.ds(pl.multiple_of(first + i * tile, tile), tile)
-        tok[0, to, :] = rms_scale(raw[at, :].astype(jnp.float32), gain_ref[...]).astype(jnp.bfloat16)
 
     @pl.when(at_end)
     def _():
@@ -293,8 +293,6 @@
             def _():
                 hid_send(b, r_at).start()
 
-        pass_down(1, far_near, 0)
-
     chunks = n * cuts
     mid = sub // 2
     here, there = 0, 1
@@ -307,9 +305,9 @@
             half_out.at[p, way], half_s, half_r.at[p], along_y if way else along_x, half_in.at[p, way]
         )
 
-    def full_copy(p, way):
+    def full_copy(p, way, part_at):
         return remote(
-            full_out.at[p, way], full_s, full_r.at[p], along_y if way else along_x, full_in.at[p, way]
+            full_out.at[p, way, part_at], full_s, full_r.at[p], along_y if way else along_x, full_in.at[p, way, part_at]
         )
 
     def source(i):
@@ -342,24 +340,27 @@
         half_out[p, 1] = across[:, mid:]
         half_copy(p, 0).start()
         half_copy(p, 1).start()
-        kept[p, there, of(x), :] = summed(p, there, x)
+        value = summed(p, there, x)
+        kept[p, there, of(x), :mid] = value[:, :mid]
+        full_out[p, 1, 1] = value[:, mid:].astype(jnp.bfloat16)
+        full_copy(p, 1, 1).start()
 
     def finish_here(at):
         p = place(at)
         pair_copy(p, here).wait_recv()
-        kept[p, here, of(1 - x), :] = summed(p, here, 1 - x)
+        value = summed(p, here, 1 - x)
+        kept[p, here, of(1 - x), mid:] = value[:, mid:]
+        full_out[p, 0, 0] = value[:, :mid].astype(jnp.bfloat16)
+        full_copy(p, 0, 0).start()
         fin[p] = summed(p, here, x)
 
     def finish_half(at):
         p = place(at)
         remote(half_in.at[p], half_s, half_r.at[p], partner).wait_recv()
-        to_x, to_y = (here, of(1 - x)), (there, of(x))
-        full_out[p, 0, :, :mid] = kept[(p, *to_x, slice(0, mid))].astype(jnp.bfloat16)
-        full_out[p, 0, :, mid:] = (kept[(p, *to_x, slice(mid, sub))] + half_in[p, 1].astype(jnp.float32)).astype(jnp.bfloat16)
-        full_copy(p, 0).start()
-        full_out[p, 1, :, mid:] = kept[(p, *to_y, slice(mid, sub))].astype(jnp.bfloat16)
-        full_out[p, 1, :, :mid] = (kept[(p, *to_y, slice(0, mid))] + half_in[p, 0].astype(jnp.float32)).astype(jnp.bfloat16)
-        full_copy(p, 1).start()
+        full_out[p, 0, 1] = (kept[p, here, of(1 - x), mid:] + half_in[p, 1].astype(jnp.float32)).astype(jnp.bfloat16)
+        full_copy(p, 0, 1).start()
+        full_out[p, 1, 0] = (kept[p, there, of(x), :mid] + half_in[p, 0].astype(jnp.float32)).astype(jnp.bfloat16)
+        full_copy(p, 1, 0).start()
 
     early = 2 * cuts
 
@@ -377,13 +378,13 @@
         def _():
             finish_there(at - 1)
 
+        @pl.when(in_middle & (at == 1))
+        def _():
+            pass_down(1, far_near, 0)
+
     @pl.when(at_end)
     def _():
         hid_wait(r)
-
-    @pl.when(in_middle)
-    def _():
-        pass_down(1, far_near, 1)
 
     @pl.loop(0, early)
     def _(at):
@@ -398,9 +399,9 @@
             finish_here(at - 1)
             finish_half(at - 1)
 
-        @pl.when(in_middle & (at == 2))
-        def _():
-            pass_down(1, far_last, 0)
+        @pl.when(in_middle & (at == 1))
+        def _():
+            pass_down(1, far_near, 1)
 
     def order(i):
         return jnp.where(in_middle & (i >= 2), jnp.where(i == 2, chunks, early + i - 1), early + i)
@@ -413,6 +414,10 @@
         def _():
             dn_wait(source(at // cuts), at % cuts)
 
+        @pl.when(in_middle & (i == 0))
+        def _():
+            pass_down(1, far_last, 0)
+
         @pl.when(in_middle & (i == 2))
         def _():
             dn_wait(far_last, cuts - 1)
@@ -436,8 +441,23 @@
         def _():
             finish_half(order(i - 1))
 
+    result = remote(res_out, res_s, res_r, outer, res_in)
+
+    def collect(at, part_at):
+        p = place(at)
+        cols = pl.ds(part_at * mid, mid)
+        both = full_in[p, 0, part_at].astype(jnp.float32) + full_in[p, 1, part_at].astype(jnp.float32)
+        return fin[p, :, cols] + both
+
+    def arrive(at):
+        remote(full_in.at[place(at)], full_s, full_r.at[place(at)], along_x).wait_recv()
+
     @pl.when(in_middle)
     def _():
+        arrive(chunks)
+        for part_at in (0, 1):
+            res_out[:, pl.ds(part_at * mid, mid)] = collect(chunks, part_at).astype(jnp.bfloat16)
+        result.start()
         finish_half(chunks - 1)
 
     remote(gu.at[:, pl.ds(0, depth)], gu_s.at[0], gu_r.at[0], inner).wait_send()
@@ -463,32 +483,23 @@
 
     squares[...] = jnp.zeros_like(squares)
 
-    result = remote(res_out, res_s, res_r, outer, res_in)
-
-    def collect(at):
-        p = place(at)
-        remote(full_in.at[p], full_s, full_r.at[p], along_x).wait_recv()
-        return fin[p] + full_in[p, 0].astype(jnp.float32) + full_in[p, 1].astype(jnp.float32)
-
-    def settle(at, total):
-        fin[place(at)] = total
-        squares[...] += total[:, :mid] * total[:, :mid] + total[:, mid:] * total[:, mid:]
+    def settle(at, part_at, total):
+        fin[place(at), :, pl.ds(part_at * mid, mid)] = total
+        squares[...] += total * total
 
     @pl.loop(0, chunks)
     def _(at):
-        @pl.when(in_middle & (at == chunks - 2))
-        def _():
-            res_out[...] = collect(chunks).astype(jnp.bfloat16)
-            result.start()
-
         @pl.when(in_middle | (at < chunks - 1))
         def _():
-            settle(at, collect(at))
+            arrive(at)
+            for part_at in (0, 1):
+                settle(at, part_at, collect(at, part_at))
 
     @pl.when(at_end)
     def _():
         result.wait_recv()
-        settle(chunks - 1, res_in[...].astype(jnp.float32))
+        for part_at in (0, 1):
+            settle(chunks - 1, part_at, res_in[:, pl.ds(part_at * mid, mid)].astype(jnp.float32))
 
     scale = lax.rsqrt(jnp.sum(squares[...], axis=-1, keepdims=True) / (n * width) + EPS)
     for p in range(chunks):
@@ -534,8 +545,8 @@
             vmem((chunks + 1, 2, 2 * rows, sub), low),
             vmem((chunks + 1, 2, rows, sub // 2), low),
             vmem((chunks + 1, 2, rows, sub // 2), low),
-            vmem((chunks + 1, 2, rows, sub), low),
-            vmem((chunks + 1, 2, rows, sub), low),
+            vmem((chunks + 1, 2, 2, rows, sub // 2), low),
+            vmem((chunks + 1, 2, 2, rows, sub // 2), low),
             vmem((chunks + 1, rows, sub), full),
             vmem((rows, sub), low),
             vmem((rows, sub), low),

time: 78 us -> 75.4 us (0.967)
  Pallas kernels: 77 us -> 74.4 us
    pallas_call x1, Pallas kernels: 77 us -> 74.4 us  [chain_body(): pl.pallas_call(functools.partial(kernel, n, rows, depth, part, width, cut...]
where the time goes in v5:
time: 75.4 us; the launch traced here: 75.2 us
  Pallas kernels  74.4 us (99%)
  local copies, waits for them, and re-layouts  0.8 us (1%)
    pallas_call x1, Pallas kernels, chain_body(): pl.pallas_call(functools.partial(kernel, n, rows, depth, part, width, cut...  74.4 us

profile of v5, /device:TPU:0, one launch (start us, length us, event | category | flops | bytes accessed | tf_op | source)
XLA Modules:
  0.0 75.2 jit_solution(5763049917609870613)
XLA Ops:
  0.0 74.4 %shard_map.64 = bf16[128,2048]{1,0:T(8,128)(2,1)S(1)} custom-call(bf16[128,2048]{1,0:T(8,128)(2,1)} %tok_ref.1, f32[1,2048]{1,0:T(1,128)} %bitcast.2, bf16[512,768]{1,0:T(8,128)(2,1)} %wg_ref.1, bf16[512,768]{1,0:T(8,128)(2,1)} %wu_ref.1, bf16[768,512]{1,0:T(8,128)(2,1)} %wd_ref.1, f32[1,2048]{1,0:T(1,128)} %bitcast.3), custom_call_target="tpu_custom_call" | custom-call | tf_op jit(solution)/shard_map/pallas_call | solution.py:532
  74.4 0.8 %copy.8 = bf16[128,2048]{1,0:T(8,128)(2,1)} copy(bf16[128,2048]{1,0:T(8,128)(2,1)S(1)} %shard_map.64) | data formatting | bytes 1048576

commit v6 on v5

--- a/solution.py
+++ b/solution.py
@@ -104,20 +104,22 @@
             ref, ref if to is None else to, send, recv, device_id=where, device_id_type=MESH
         )
 
-    def gu_at(s, b):
-        return gu.at[b, pl.ds(pl.multiple_of(s * depth, depth), depth)]
-
-    def gu_send(kind, b):
-        return remote(
-            gu_at(last if kind else k, b), gu_s.at[kind], gu_r.at[b + jnp.where(in_middle, blocks, 0)], inner
-        )
-
-    def gu_pass(b):
-        remote(gu_at(last, b), gu_s.at[1], gu_r.at[b], inner).wait_recv()
-        gu_send(1, b).start()
+    pieces = 2
+    step_depth = depth // pieces
+
+    def gu_at(s, b, h):
+        return gu.at[b, pl.ds(pl.multiple_of(s * depth + h * step_depth, step_depth), step_depth)]
+
+    def gu_send(kind, b, h):
+        at = jnp.where(in_middle, pieces * blocks + b, pieces * b + h)
+        return remote(gu_at(last if kind else k, b, h), gu_s.at[kind], gu_r.at[at], inner)
+
+    def gu_pass(b, h):
+        remote(gu_at(last, b, h), gu_s.at[1], gu_r.at[pieces * b + h], inner).wait_recv()
+        gu_send(1, b, h).start()
 
     def gu_wait(b):
-        remote(gu.at[b, pl.ds(0, 2 * depth)], gu_s.at[0], gu_r.at[blocks + b], inner).wait_recv()
+        remote(gu.at[b, pl.ds(0, 2 * depth)], gu_s.at[0], gu_r.at[pieces * blocks + b], inner).wait_recv()
 
     def dn_send(way, s, j):
         at = s * cuts + j
@@ -191,7 +193,8 @@
     def send_own_gu():
         for b in range(blocks):
             pltpu.make_async_copy(gu.at[b, own_depth], gu.at[b, own_depth], gu_l.at[b]).wait()
-            gu_send(0, b).start()
+            for h in range(pieces):
+                gu_send(0, b, h).start()
 
     def send_own_dn(way):
         own = dn.at[pl.ds(k * cuts, cuts)]
@@ -238,29 +241,33 @@
                 go(1, 13, 3, 7, 8, 9)
                 got(1, 6)
                 go(1, 10)
+                gu_pass(0, 0)
                 got(1, 7)
                 go(1, 17, 11)
                 got(1, 2, 3)
                 go(1, 15)
-                gu_pass(0)
+                gu_pass(0, 1)
                 go(0, 2, 4)
-                gu_pass(1)
+                gu_pass(1, 0)
+                go(0, 3, 5)
                 got(1, 8, 9)
                 go(1, 18)
                 got(1, 10, 11)
                 go(1, 19)
-                go(0, 3, 5, 8, 10)
+                go(0, 8, 10)
+                gu_pass(1, 1)
                 got(1, 12, 13, 14, 15, 16, 17, 18, 19)
                 gu_wait(0)
 
             @step(2)
             def _():
                 go(0, 9, 11)
+                gu_pass(2, 0)
                 got(0, 2, 3)
                 go(0, 15)
                 got(0, 4, 5)
                 go(0, 16)
-                gu_pass(2)
+                gu_pass(2, 1)
                 gu_wait(1)
 
             @step(4)
@@ -275,6 +282,9 @@
                 got(0, 10, 11)
                 go(0, 19)
                 gu_wait(2)
+
+            @pl.when(at_step == 6 + c)
+            def _():
                 for j in range(cuts):
                     dn_send(0, k, j).start()
                 dn_send(0, last, 0).start()
@@ -399,9 +409,6 @@
             finish_here(at - 1)
             finish_half(at - 1)
 
-        @pl.when(in_middle & (at == 1))
-        def _():
-            pass_down(1, far_near, 1)
 
     def order(i):
         return jnp.where(in_middle & (i >= 2), jnp.where(i == 2, chunks, early + i - 1), early + i)
@@ -415,6 +422,10 @@
             dn_wait(source(at // cuts), at % cuts)
 
         @pl.when(in_middle & (i == 0))
+        def _():
+            pass_down(1, far_near, 1)
+
+        @pl.when(in_middle & (i == 1))
         def _():
             pass_down(1, far_last, 0)
 
@@ -559,7 +570,7 @@
             dma((2,)),
             dma((2, 8)),
             dma((2,)),
-            dma((2 * blocks,)),
+            dma((3 * blocks,)),
             dma((2,)),
             dma((chunks,)),
             dma(()),

time: 75.4 us -> 73.5 us (0.975)
  Pallas kernels: 74.4 us -> 72.5 us
    pallas_call x1, Pallas kernels: 74.4 us -> 72.5 us  [chain_body(): pl.pallas_call(functools.partial(kernel, n, rows, depth, part, width, cut...]
where the time goes in v6:
time: 73.5 us; the launch traced here: 73.3 us
  Pallas kernels  72.5 us (99%)
  local copies, waits for them, and re-layouts  0.8 us (1%)
    pallas_call x1, Pallas kernels, chain_body(): pl.pallas_call(functools.partial(kernel, n, rows, depth, part, width, cut...  72.5 us

profile of v6, /device:TPU:0, one launch (start us, length us, event | category | flops | bytes accessed | tf_op | source)
XLA Modules:
  0.0 73.3 jit_solution(2695771358804001535)
XLA Ops:
  0.0 72.5 %shard_map.64 = bf16[128,2048]{1,0:T(8,128)(2,1)S(1)} custom-call(bf16[128,2048]{1,0:T(8,128)(2,1)} %tok_ref.1, f32[1,2048]{1,0:T(1,128)} %bitcast.2, bf16[512,768]{1,0:T(8,128)(2,1)} %wg_ref.1, bf16[512,768]{1,0:T(8,128)(2,1)} %wu_ref.1, bf16[768,512]{1,0:T(8,128)(2,1)} %wd_ref.1, f32[1,2048]{1,0:T(1,128)} %bitcast.3), custom_call_target="tpu_custom_call" | custom-call | tf_op jit(solution)/shard_map/pallas_call | solution.py:543
  72.5 0.8 %copy.8 = bf16[128,2048]{1,0:T(8,128)(2,1)} copy(bf16[128,2048]{1,0:T(8,128)(2,1)S(1)} %shard_map.64) | data formatting | bytes 1048576

commit v7 on v6

--- a/solution.py
+++ b/solution.py
@@ -39,9 +39,9 @@
 def kernel(
     n, rows, depth, part, width, cuts, lanes,
     tok_ref, gain_ref, wg_ref, wu_ref, wd_ref, post_ref, out_ref,
-    raw, tok, gu, dn, hid, kept, pair_out, pair_in, half_out, half_in, full_out, full_in, fin, res_out, res_in, squares,
+    raw, tok, gu, dn, hid, kept, pair_out, pair_in, half_out, half_in, full_out, full_in, fin, res_out, res_in, diag_out, diag_in, squares,
     tok_l, gu_l, dn_l, z_s, z_r, tok_s, tok_r, gu_s, gu_r, dn_s, dn_r, hid_s, hid_r,
-    pair_s, pair_r, half_s, half_r, full_s, full_r, res_s, res_r,
+    pair_s, pair_r, half_s, half_r, full_s, full_r, res_s, res_r, diag_s, diag_r,
 ):
     r, k, t = lax.axis_index("rep"), lax.axis_index("fs"), lax.axis_index("tp")
     x, c = t // 2, t % 2
@@ -152,7 +152,7 @@
     )
     groups = (
         ((0, 1), (6, 7), (2, 3), (4, 5), (8, 9), (10, 11), (12, 13, 14, 15), (16, 17, 18, 19)),
-        ((0, 4), (1, 5), (6,), (7,), (2, 3), (8, 9), (10, 11), (12, 13, 14, 15, 16, 17, 18, 19)),
+        ((0, 4), (1, 5), (6,), (7,), (2, 3), (8, 9), (10, 11), (12, 13, 14, 15), (16, 17, 18, 19)),
     )
 
     def group_of(p, i):
@@ -189,6 +189,39 @@
         both = jnp.dot(tok[p, half_rows(r_at), :], gu[b], preferred_element_type=jnp.float32)
         gate, up = both[:, :lanes], both[:, lanes:]
         hid_at(p, b, r_at)[...] = (gate / (1.0 + jnp.exp(-gate)) * up).astype(jnp.bfloat16)
+
+    chunks = n * cuts
+    mid = sub // 2
+    here, there = 0, 1
+
+    def pair_copy(p, side):
+        return remote(pair_out.at[p, side], pair_s, pair_r.at[p, side], partner, pair_in.at[p, side])
+
+    def half_copy(p, way):
+        return remote(
+            half_out.at[p, way], half_s, half_r.at[p], along_y if way else along_x, half_in.at[p, way]
+        )
+
+    def full_copy(p, way, part_at):
+        return remote(
+            full_out.at[p, way, part_at], full_s, full_r.at[p], along_y if way else along_x, full_in.at[p, way, part_at]
+        )
+
+    def source(i):
+        near_or_last = jnp.where(i == 0, k, near + last - k)
+        return jnp.where(i < 2, near_or_last, jnp.where(i == 2, far_near, far_last))
+
+    def place(at):
+        return jnp.where(at < chunks, source(at // cuts) * cuts + at % cuts, chunks)
+
+    def product(at, side):
+        p = place(at)
+        held = jnp.where(at < chunks, p, far_last * cuts + cuts - 1)
+        rows_at = half_rows(r_y if side == there else r)
+        both = jnp.dot(hid[jnp.where(at < chunks, 0, 1), rows_at, :], dn[held], preferred_element_type=jnp.float32)
+        pair_out[p, side] = both[quarter:].astype(jnp.bfloat16)
+        pair_copy(p, side).start()
+        kept[p, side] = both[:quarter]
 
     def send_own_gu():
         for b in range(blocks):
@@ -256,18 +289,33 @@
                 go(1, 19)
                 go(0, 8, 10)
                 gu_pass(1, 1)
-                got(1, 12, 13, 14, 15, 16, 17, 18, 19)
+                got(1, 12, 13, 14, 15)
                 gu_wait(0)
 
+            @step(1)
+            def _():
+                got(1, 16, 17, 18, 19)
+
+            @pl.when(at_step == 2 - c)
+            def _():
+                gu_pass(2, 0)
+
             @step(2)
             def _():
                 go(0, 9, 11)
-                gu_pass(2, 0)
                 got(0, 2, 3)
                 go(0, 15)
                 got(0, 4, 5)
                 go(0, 16)
                 gu_pass(2, 1)
+
+            @pl.when(at_step == 2 + 4 * c)
+            def _():
+                for j in range(cuts):
+                    dn_send(0, k, j).start()
+
+            @step(2)
+            def _():
                 gu_wait(1)
 
             @step(4)
@@ -276,65 +324,33 @@
 
             @step(6)
             def _():
-                dn_wait(last, 0)
+                pass_down(0, last, 0)
                 got(0, 8, 9)
                 go(0, 18)
                 got(0, 10, 11)
                 go(0, 19)
                 gu_wait(2)
 
-            @pl.when(at_step == 6 + c)
-            def _():
-                for j in range(cuts):
-                    dn_send(0, k, j).start()
-                dn_send(0, last, 0).start()
-
-            @step(9)
-            def _():
+            @step(8)
+            def _():
+                got(0, 16, 17, 18, 19)
+
+            @step(11)
+            def _():
+                pl.loop(0, 2)(lambda at: product(at, there))
                 pass_down(0, last, 1)
-                got(0, 16, 17, 18, 19)
 
             passed = (at_step < 4) | (at_step == 6) | (at_step == 7)
-            b = jnp.where(at_step < 4, at_step // 2, jnp.where(at_step < 6, at_step - 4, jnp.where(at_step < 9, 2, at_step - 9)))
-            r_at = jnp.where(passed, (r_y + at_step % 2) % 2, jnp.where(at_step < 9, r, r_y))
+            late = jnp.where(at_step < 8, 2, jnp.where(at_step < 11, at_step - 8, 2))
+            b = jnp.where(at_step < 4, at_step // 2, jnp.where(at_step < 6, at_step - 4, late))
+            first_r = jnp.where(at_step < 2, r, r_y)
+            own_r = jnp.where((at_step < 6) | (at_step == 11), r, r_y)
+            r_at = jnp.where(passed, (first_r + at_step % 2) % 2, own_r)
             gated(jnp.where(passed, 1, 0), b, r_at)
 
             @pl.when(passed)
             def _():
                 hid_send(b, r_at).start()
-
-    chunks = n * cuts
-    mid = sub // 2
-    here, there = 0, 1
-
-    def pair_copy(p, side):
-        return remote(pair_out.at[p, side], pair_s, pair_r.at[p, side], partner, pair_in.at[p, side])
-
-    def half_copy(p, way):
-        return remote(
-            half_out.at[p, way], half_s, half_r.at[p], along_y if way else along_x, half_in.at[p, way]
-        )
-
-    def full_copy(p, way, part_at):
-        return remote(
-            full_out.at[p, way, part_at], full_s, full_r.at[p], along_y if way else along_x, full_in.at[p, way, part_at]
-        )
-
-    def source(i):
-        near_or_last = jnp.where(i == 0, k, near + last - k)
-        return jnp.where(i < 2, near_or_last, jnp.where(i == 2, far_near, far_last))
-
-    def place(at):
-        return jnp.where(at < chunks, source(at // cuts) * cuts + at % cuts, chunks)
-
-    def product(at, side):
-        p = place(at)
-        held = jnp.where(at < chunks, p, far_last * cuts + cuts - 1)
-        rows_at = half_rows(r_y if side == there else r)
-        both = jnp.dot(hid[jnp.where(at < chunks, 0, 1), rows_at, :], dn[held], preferred_element_type=jnp.float32)
-        pair_out[p, side] = both[quarter:].astype(jnp.bfloat16)
-        pair_copy(p, side).start()
-        kept[p, side] = both[:quarter]
 
     def of(m):
         return pl.ds(pl.multiple_of(m * rows, rows), rows)
@@ -364,6 +380,24 @@
         full_copy(p, 0, 0).start()
         fin[p] = summed(p, here, x)
 
+    across_copy = remote(diag_out, diag_s, diag_r, diag, diag_in)
+
+    def finish_direct(at):
+        p = place(at)
+        pair_copy(p, there).wait_recv()
+        diag_out[...] = summed(p, there, 1 - x).astype(jnp.bfloat16)
+        across_copy.start()
+        value = summed(p, there, x).astype(jnp.bfloat16)
+        for part_at in (1, 0):
+            full_out[p, 1, part_at] = value[:, part_at * mid : (part_at + 1) * mid]
+            full_copy(p, 1, part_at).start()
+        pair_copy(p, here).wait_recv()
+        value = summed(p, here, 1 - x).astype(jnp.bfloat16)
+        for part_at in (0, 1):
+            full_out[p, 0, part_at] = value[:, part_at * mid : (part_at + 1) * mid]
+            full_copy(p, 0, part_at).start()
+        fin[p] = summed(p, here, x)
+
     def finish_half(at):
         p = place(at)
         remote(half_in.at[p], half_s, half_r.at[p], partner).wait_recv()
@@ -382,13 +416,15 @@
 
     @pl.loop(0, early)
     def _(at):
-        product(at, there)
+        @pl.when(at_end | (at > 1))
+        def _():
+            product(at, there)
 
         @pl.when(at > 0)
         def _():
             finish_there(at - 1)
 
-        @pl.when(in_middle & (at == 1))
+        @pl.when(in_middle & (at == 0))
         def _():
             pass_down(1, far_near, 0)
 
@@ -409,6 +445,10 @@
             finish_here(at - 1)
             finish_half(at - 1)
 
+        @pl.when(in_middle & (at == 2))
+        def _():
+            pass_down(1, far_near, 1)
+
 
     def order(i):
         return jnp.where(in_middle & (i >= 2), jnp.where(i == 2, chunks, early + i - 1), early + i)
@@ -423,10 +463,6 @@
 
         @pl.when(in_middle & (i == 0))
         def _():
-            pass_down(1, far_near, 1)
-
-        @pl.when(in_middle & (i == 1))
-        def _():
             pass_down(1, far_last, 0)
 
         @pl.when(in_middle & (i == 2))
@@ -443,12 +479,16 @@
             finish_here(early - 1)
             finish_half(early - 1)
 
-        @pl.when(in_middle | (i < 3))
+        @pl.when(in_middle | (i < 2))
         def _():
             finish_there(at)
             finish_here(at)
 
-        @pl.when((i > 0) & (in_middle | (i < 4)))
+        @pl.when(at_end & (i == 2))
+        def _():
+            finish_direct(at)
+
+        @pl.when((i > 0) & (in_middle | (i < 3)))
         def _():
             finish_half(order(i - 1))
 
@@ -478,7 +518,8 @@
         remote(tok.at[0, pl.ds(0, rows)], z_s, z_r.at[0], inner).wait_send()
         remote(dn.at[pl.ds(0, cuts)], dn_s.at[0], dn_r.at[0], inner).wait_send()
         remote(pair_out.at[pl.ds(0, chunks - 1)], pair_s, pair_r.at[0, 0], partner).wait_send()
-        remote(half_out.at[pl.ds(0, chunks - 1)], half_s, half_r.at[0], along_x).wait_send()
+        remote(half_out.at[pl.ds(0, chunks - 2)], half_s, half_r.at[0], along_x).wait_send()
+        across_copy.wait_send()
 
     @pl.when(in_middle)
     def _():
@@ -500,7 +541,7 @@
 
     @pl.loop(0, chunks)
     def _(at):
-        @pl.when(in_middle | (at < chunks - 1))
+        @pl.when(in_middle | (at < chunks - 2))
         def _():
             arrive(at)
             for part_at in (0, 1):
@@ -508,6 +549,14 @@
 
     @pl.when(at_end)
     def _():
+        across_copy.wait_recv()
+        p = place(chunks - 2)
+        for part_at in (0, 1):
+            cols = pl.ds(part_at * mid, mid)
+            fin[p, :, cols] = fin[p, :, cols] + diag_in[:, cols].astype(jnp.float32)
+        arrive(chunks - 2)
+        for part_at in (0, 1):
+            settle(chunks - 2, part_at, collect(chunks - 2, part_at))
         result.wait_recv()
         for part_at in (0, 1):
             settle(chunks - 1, part_at, res_in[:, pl.ds(part_at * mid, mid)].astype(jnp.float32))
@@ -561,6 +610,8 @@
             vmem((chunks + 1, rows, sub), full),
             vmem((rows, sub), low),
             vmem((rows, sub), low),
+            vmem((rows, sub), low),
+            vmem((rows, sub), low),
             vmem((rows, sub // 2), full),
             dma(()),
             dma((blocks,)),
@@ -568,7 +619,7 @@
             dma(()),
             dma((4,)),
             dma((2,)),
-            dma((2, 8)),
+            dma((2, 9)),
             dma((2,)),
             dma((3 * blocks,)),
             dma((2,)),
@@ -581,6 +632,8 @@
             dma((chunks + 1,)),
             dma(()),
             dma((chunks + 1,)),
+            dma(()),
+            dma(()),
             dma(()),
             dma(()),
         ],

time: 73.5 us -> 72.4 us (0.985)
  Pallas kernels: 72.5 us -> 71.4 us
    pallas_call x1, Pallas kernels: 72.5 us -> 71.4 us  [chain_body(): pl.pallas_call(functools.partial(kernel, n, rows, depth, part, width, cut...]
where the time goes in v7:
time: 72.4 us; the launch traced here: 72.2 us
  Pallas kernels  71.4 us (99%)
  local copies, waits for them, and re-layouts  0.8 us (1%)
    pallas_call x1, Pallas kernels, chain_body(): pl.pallas_call(functools.partial(kernel, n, rows, depth, part, width, cut...  71.4 us

profile of v7, /device:TPU:0, one launch (start us, length us, event | category | flops | bytes accessed | tf_op | source)
XLA Modules:
  0.0 72.2 jit_solution(18186523033167043216)
XLA Ops:
  0.0 71.4 %shard_map.64 = bf16[128,2048]{1,0:T(8,128)(2,1)S(1)} custom-call(bf16[128,2048]{1,0:T(8,128)(2,1)} %tok_ref.1, f32[1,2048]{1,0:T(1,128)} %bitcast.2, bf16[512,768]{1,0:T(8,128)(2,1)} %wg_ref.1, bf16[512,768]{1,0:T(8,128)(2,1)} %wu_ref.1, bf16[768,512]{1,0:T(8,128)(2,1)} %wd_ref.1, f32[1,2048]{1,0:T(1,128)} %bitcast.3), custom_call_target="tpu_custom_call" | custom-call | tf_op jit(solution)/shard_map/pallas_call | solution.py:592
  71.4 0.8 %copy.8 = bf16[128,2048]{1,0:T(8,128)(2,1)} copy(bf16[128,2048]{1,0:T(8,128)(2,1)S(1)} %shard_map.64) | data formatting | bytes 1048576

commit v8 on v7

--- a/solution.py
+++ b/solution.py
@@ -180,10 +180,12 @@
         return hid.at[p, half_rows(r_at), pl.ds(pl.multiple_of(b * lanes, lanes), lanes)]
 
     def hid_send(b, r_at):
-        return remote(hid_at(1, b, r_at), hid_s, hid_r.at[r_at], outer, hid_at(0, b, r_at))
-
-    def hid_wait(r_at):
-        remote(hid.at[0, half_rows(r_at)], hid_s, hid_r.at[r_at], partner).wait_recv()
+        sem = jnp.where((b == 0) & (r_at == r), 2, r_at)
+        return remote(hid_at(1, b, r_at), hid_s, hid_r.at[sem], outer, hid_at(0, b, r_at))
+
+    def hid_wait(r_at, first, count, sem):
+        held = hid.at[0, half_rows(r_at), pl.ds(first * lanes, count * lanes)]
+        remote(held, hid_s, hid_r.at[sem], partner).wait_recv()
 
     def gated(p, b, r_at):
         both = jnp.dot(tok[p, half_rows(r_at), :], gu[b], preferred_element_type=jnp.float32)
@@ -245,6 +247,7 @@
         for i in range(4):
             z_send(i).start()
         send_own_gu()
+        hid_wait(r, 0, 1, 2)
         send_own_dn(0)
 
     @pl.when(in_middle)
@@ -324,7 +327,6 @@
 
             @step(6)
             def _():
-                pass_down(0, last, 0)
                 got(0, 8, 9)
                 go(0, 18)
                 got(0, 10, 11)
@@ -334,6 +336,10 @@
             @step(8)
             def _():
                 got(0, 16, 17, 18, 19)
+
+            @step(10)
+            def _():
+                pass_down(0, last, 0)
 
             @step(11)
             def _():
@@ -412,7 +418,7 @@
     def _():
         for j in range(cuts):
             dn_wait(near, j)
-        hid_wait(r_y)
+        hid_wait(r_y, 0, blocks, r_y)
 
     @pl.loop(0, early)
     def _(at):
@@ -430,7 +436,7 @@
 
     @pl.when(at_end)
     def _():
-        hid_wait(r)
+        hid_wait(r, 1, blocks - 1, r)
 
     @pl.loop(0, early)
     def _(at):
@@ -449,48 +455,6 @@
         def _():
             pass_down(1, far_near, 1)
 
-
-    def order(i):
-        return jnp.where(in_middle & (i >= 2), jnp.where(i == 2, chunks, early + i - 1), early + i)
-
-    @pl.loop(0, chunks - early + 1)
-    def _(i):
-        at = order(i)
-
-        @pl.when(at_end & (i < 3))
-        def _():
-            dn_wait(source(at // cuts), at % cuts)
-
-        @pl.when(in_middle & (i == 0))
-        def _():
-            pass_down(1, far_last, 0)
-
-        @pl.when(in_middle & (i == 2))
-        def _():
-            dn_wait(far_last, cuts - 1)
-
-        @pl.when(in_middle | (i < 3))
-        def _():
-            product(at, there)
-            product(at, here)
-
-        @pl.when(i == 0)
-        def _():
-            finish_here(early - 1)
-            finish_half(early - 1)
-
-        @pl.when(in_middle | (i < 2))
-        def _():
-            finish_there(at)
-            finish_here(at)
-
-        @pl.when(at_end & (i == 2))
-        def _():
-            finish_direct(at)
-
-        @pl.when((i > 0) & (in_middle | (i < 3)))
-        def _():
-            finish_half(order(i - 1))
 
     result = remote(res_out, res_s, res_r, outer, res_in)
 
@@ -503,12 +467,61 @@
     def arrive(at):
         remote(full_in.at[place(at)], full_s, full_r.at[place(at)], along_x).wait_recv()
 
+    def order(i):
+        return jnp.where(in_middle & (i >= 2), jnp.where(i == 2, chunks, early + i - 1), early + i)
+
+    @pl.loop(0, chunks - early + 1)
+    def _(i):
+        at = order(i)
+
+        @pl.when(at_end & (i < 3))
+        def _():
+            dn_wait(source(at // cuts), at % cuts)
+
+        @pl.when(in_middle & (i == 1 * c))
+        def _():
+            pass_down(1, far_last, 0)
+
+        @pl.when(in_middle & (i == 2))
+        def _():
+            dn_wait(far_last, cuts - 1)
+
+        @pl.when(in_middle | (i < 3))
+        def _():
+            product(at, there)
+            product(at, here)
+
+        @pl.when(i == 0)
+        def _():
+            finish_here(early - 1)
+            finish_half(early - 1)
+
+        @pl.when(in_middle & (i == 3))
+        def _():
+            finish_half(chunks)
+
+        @pl.when(in_middle | (i < 2))
+        def _():
+            finish_there(at)
+            finish_here(at)
+
+        @pl.when(at_end & (i == 2))
+        def _():
+            finish_direct(at)
+
+        @pl.when(in_middle & (i == 4))
+        def _():
+            arrive(chunks)
+            for part_at in (0, 1):
+                res_out[:, pl.ds(part_at * mid, mid)] = collect(chunks, part_at).astype(jnp.bfloat16)
+            result.start()
+
+        @pl.when((i > 0) & (i != 3) & (in_middle | (i < 3)))
+        def _():
+            finish_half(order(i - 1))
+
     @pl.when(in_middle)
     def _():
-        arrive(chunks)
-        for part_at in (0, 1):
-            res_out[:, pl.ds(part_at * mid, mid)] = collect(chunks, part_at).astype(jnp.bfloat16)
-        result.start()
         finish_half(chunks - 1)
 
     remote(gu.at[:, pl.ds(0, depth)], gu_s.at[0], gu_r.at[0], inner).wait_send()
@@ -625,7 +638,7 @@
             dma((2,)),
             dma((chunks,)),
             dma(()),
-            dma((2,)),
+            dma((3,)),
             dma(()),
             dma((chunks + 1, 2)),
             dma(()),

time: 72.4 us -> 71.4 us (0.986)
  Pallas kernels: 71.4 us -> 70.4 us
    pallas_call x1, Pallas kernels: 71.4 us -> 70.4 us  [chain_body(): pl.pallas_call(functools.partial(kernel, n, rows, depth, part, width, cut...]
where the time goes in v8:
time: 71.4 us; the launch traced here: 71.2 us
  Pallas kernels  70.4 us (99%)
  local copies, waits for them, and re-layouts  0.8 us (1%)
    pallas_call x1, Pallas kernels, chain_body(): pl.pallas_call(functools.partial(kernel, n, rows, depth, part, width, cut...  70.4 us

profile of v8, /device:TPU:0, one launch (start us, length us, event | category | flops | bytes accessed | tf_op | source)
XLA Modules:
  0.0 71.2 jit_solution(655620975519824934)
XLA Ops:
  0.0 70.4 %shard_map.64 = bf16[128,2048]{1,0:T(8,128)(2,1)S(1)} custom-call(bf16[128,2048]{1,0:T(8,128)(2,1)} %tok_ref.1, f32[1,2048]{1,0:T(1,128)} %bitcast.2, bf16[512,768]{1,0:T(8,128)(2,1)} %wg_ref.1, bf16[512,768]{1,0:T(8,128)(2,1)} %wu_ref.1, bf16[768,512]{1,0:T(8,128)(2,1)} %wd_ref.1, f32[1,2048]{1,0:T(1,128)} %bitcast.3), custom_call_target="tpu_custom_call" | custom-call | tf_op jit(solution)/shard_map/pallas_call | solution.py:605
  70.4 0.8 %copy.8 = bf16[128,2048]{1,0:T(8,128)(2,1)} copy(bf16[128,2048]{1,0:T(8,128)(2,1)S(1)} %shard_map.64) | data formatting | bytes 1048576

commit v9 on v8

--- a/solution.py
+++ b/solution.py
@@ -39,8 +39,8 @@
 def kernel(
     n, rows, depth, part, width, cuts, lanes,
     tok_ref, gain_ref, wg_ref, wu_ref, wd_ref, post_ref, out_ref,
-    raw, tok, gu, dn, hid, kept, pair_out, pair_in, half_out, half_in, full_out, full_in, fin, res_out, res_in, diag_out, diag_in, squares,
-    tok_l, gu_l, dn_l, z_s, z_r, tok_s, tok_r, gu_s, gu_r, dn_s, dn_r, hid_s, hid_r,
+    gain, post, raw, tok, gu, dn, hid, kept, pair_out, pair_in, half_out, half_in, full_out, full_in, fin, res_out, res_in, diag_out, diag_in, squares,
+    gain_l, post_l, tok_l, gu_l, dn_l, z_s, z_r, tok_s, tok_r, gu_s, gu_r, dn_s, dn_r, hid_s, hid_r,
     pair_s, pair_r, half_s, half_r, full_s, full_r, res_s, res_r, diag_s, diag_r,
 ):
     r, k, t = lax.axis_index("rep"), lax.axis_index("fs"), lax.axis_index("tp")
@@ -71,13 +71,17 @@
         return pltpu.make_async_copy(wd_ref.at[pl.ds(half, part), pl.ds(j * sub, sub)], dn.at[k * cuts + j], dn_l)
 
     tok_load = pltpu.make_async_copy(tok_ref, raw, tok_l)
+    gain_load = pltpu.make_async_copy(gain_ref, gain, gain_l)
+    post_load = pltpu.make_async_copy(post_ref, post, post_l)
 
     tok_load.start()
+    gain_load.start()
     for b in range(blocks):
         for q in (0, 1):
             gu_load(b, q).start()
     for j in range(cuts):
         dn_load(j).start()
+    post_load.start()
 
     barrier = pltpu.get_barrier_semaphore()
     for where in (partner, along_x, along_y, diag, inner):
@@ -88,6 +92,7 @@
         pl.semaphore_signal(barrier, inc=1, device_id=outer, device_id_type=MESH)
 
     tok_load.wait()
+    gain_load.wait()
     tile = 32
     first = (r * 4 + x) * rows
 
@@ -95,7 +100,7 @@
     def _(i):
         at = pl.ds(pl.multiple_of(i * tile, tile), tile)
         to = pl.ds(pl.multiple_of(first + i * tile, tile), tile)
-        tok[0, to, :] = rms_scale(raw[at, :].astype(jnp.float32), gain_ref[...]).astype(jnp.bfloat16)
+        tok[0, to, :] = rms_scale(raw[at, :].astype(jnp.float32), gain[...]).astype(jnp.bfloat16)
 
     pl.semaphore_wait(barrier, 5 + jnp.where(in_middle, 1, 0))
 
@@ -478,7 +483,7 @@
         def _():
             dn_wait(source(at // cuts), at % cuts)
 
-        @pl.when(in_middle & (i == 1 * c))
+        @pl.when(in_middle & (i == 0) & (c == 0))
         def _():
             pass_down(1, far_last, 0)
 
@@ -508,6 +513,10 @@
         @pl.when(at_end & (i == 2))
         def _():
             finish_direct(at)
+
+        @pl.when(in_middle & (i == 1) & (c == 1))
+        def _():
+            pass_down(1, far_last, 0)
 
         @pl.when(in_middle & (i == 4))
         def _():
@@ -574,10 +583,11 @@
         for part_at in (0, 1):
             settle(chunks - 1, part_at, res_in[:, pl.ds(part_at * mid, mid)].astype(jnp.float32))
 
+    post_load.wait()
     scale = lax.rsqrt(jnp.sum(squares[...], axis=-1, keepdims=True) / (n * width) + EPS)
     for p in range(chunks):
         cols = pl.ds(p * sub, sub)
-        out_ref[:, cols] = (fin[p] * scale * post_ref[:, cols]).astype(out_ref.dtype)
+        out_ref[:, cols] = (fin[p] * scale * post[:, cols]).astype(out_ref.dtype)
 
     @pl.when(at_end)
     def _():
@@ -605,9 +615,11 @@
     return pl.pallas_call(
         functools.partial(kernel, n, rows, depth, part, width, cuts, LANES),
         out_shape=pltpu.VMEM((rows, model), low),
-        in_specs=[anywhere, inside, anywhere, anywhere, anywhere, inside],
+        in_specs=[anywhere] * 6,
         out_specs=inside,
         scratch_shapes=[
+            vmem((1, model), full),
+            vmem((1, model), full),
             vmem((rows, model), low),
             vmem((2, 8 * rows, model), low),
             vmem((blocks, n * depth, 2 * LANES), low),
@@ -627,6 +639,8 @@
             vmem((rows, sub), low),
             vmem((rows, sub // 2), full),
             dma(()),
+            dma(()),
+            dma(()),
             dma((blocks,)),
             dma(()),
             dma(()),

time: 71.4 us -> 71 us (level)
  no operation moved by 1% of the time
where the time goes in v9:
time: 71 us; the launch traced here: 70.9 us
  Pallas kernels  70.1 us (99%)
  local copies, waits for them, and re-layouts  0.8 us (1%)
    pallas_call x1, Pallas kernels, chain_body(): pl.pallas_call(functools.partial(kernel, n, rows, depth, part, width, cut...  70.1 us

profile of v9, /device:TPU:0, one launch (start us, length us, event | category | flops | bytes accessed | tf_op | source)
XLA Modules:
  0.0 70.9 jit_solution(10580874226105327901)
XLA Ops:
  0.0 70.1 %shard_map.64 = bf16[128,2048]{1,0:T(8,128)(2,1)S(1)} custom-call(bf16[128,2048]{1,0:T(8,128)(2,1)} %tok_ref.1, f32[1,2048]{1,0:T(1,128)} %bitcast.2, bf16[512,768]{1,0:T(8,128)(2,1)} %wg_ref.1, bf16[512,768]{1,0:T(8,128)(2,1)} %wu_ref.1, bf16[768,512]{1,0:T(8,128)(2,1)} %wd_ref.1, f32[1,2048]{1,0:T(1,128)} %bitcast.3), custom_call_target="tpu_custom_call" | custom-call | tf_op jit(solution)/shard_map/pallas_call | solution.py:615
  70.1 0.8 %copy.8 = bf16[128,2048]{1,0:T(8,128)(2,1)} copy(bf16[128,2048]{1,0:T(8,128)(2,1)S(1)} %shard_map.64) | data formatting | bytes 1048576

commit v10 on v9

--- a/solution.py
+++ b/solution.py
@@ -40,8 +40,8 @@
     n, rows, depth, part, width, cuts, lanes,
     tok_ref, gain_ref, wg_ref, wu_ref, wd_ref, post_ref, out_ref,
     gain, post, raw, tok, gu, dn, hid, kept, pair_out, pair_in, half_out, half_in, full_out, full_in, fin, res_out, res_in, diag_out, diag_in, squares,
-    gain_l, post_l, tok_l, gu_l, dn_l, z_s, z_r, tok_s, tok_r, gu_s, gu_r, dn_s, dn_r, hid_s, hid_r,
-    pair_s, pair_r, half_s, half_r, full_s, full_r, res_s, res_r, diag_s, diag_r,
+    gain_l, post_l, tok_l, gu_l, dn_l, z_s, z_r, tok_s, tok_r, gu_s, gu_r, dn_s, dn_r,
+    pair_s, pair_r, half_s, half_r, full_s, full_r, res_s,
 ):
     r, k, t = lax.axis_index("rep"), lax.axis_index("fs"), lax.axis_index("tp")
     x, c = t // 2, t % 2
@@ -76,20 +76,21 @@
 
     tok_load.start()
     gain_load.start()
+
+    barrier = pltpu.get_barrier_semaphore()
+    for where in (partner, along_x, along_y, diag, inner):
+        pl.semaphore_signal(barrier, inc=1, device_id=where, device_id_type=MESH)
+
+    @pl.when(in_middle)
+    def _():
+        pl.semaphore_signal(barrier, inc=1, device_id=outer, device_id_type=MESH)
+
     for b in range(blocks):
         for q in (0, 1):
             gu_load(b, q).start()
     for j in range(cuts):
         dn_load(j).start()
     post_load.start()
-
-    barrier = pltpu.get_barrier_semaphore()
-    for where in (partner, along_x, along_y, diag, inner):
-        pl.semaphore_signal(barrier, inc=1, device_id=where, device_id_type=MESH)
-
-    @pl.when(in_middle)
-    def _():
-        pl.semaphore_signal(barrier, inc=1, device_id=outer, device_id_type=MESH)
 
     tok_load.wait()
     gain_load.wait()
@@ -156,8 +157,8 @@
         + [((r_at, t_at, i, 2), partner) for r_at, t_at in ((r, t), (r, t_x), (r_y, t), (r_y, t_x)) for i in (0, 2)]
     )
     groups = (
-        ((0, 1), (6, 7), (2, 3), (4, 5), (8, 9), (10, 11), (12, 13, 14, 15), (16, 17, 18, 19)),
-        ((0, 4), (1, 5), (6,), (7,), (2, 3), (8, 9), (10, 11), (12, 13, 14, 15), (16, 17, 18, 19)),
+        ((0, 1, 6, 7), (2, 3, 4, 5), (8, 9, 10, 11), (12, 13, 14, 15), (16, 17, 18, 19)),
+        ((0, 4), (1, 5), (6,), (2, 3, 7), (8, 9, 10, 11), (12, 13, 14, 15), (16, 17, 18, 19)),
     )
 
     def group_of(p, i):
@@ -167,13 +168,13 @@
         for i in which:
             at, where = sends[i]
             to = rows_of(p, *at, 1 - c if i >= 12 else c)
-            remote(rows_of(p, *at, c), tok_s.at[p], tok_r.at[p, group_of(p, i)], where, to).start()
+            remote(rows_of(p, *at, c), tok_s.at[p], tok_r.at[5 * p + group_of(p, i)], where, to).start()
 
     def got(p, *which):
         g = group_of(p, which[0])
         assert groups[p][g] == which
         count = sum(1 if i < 12 else 2 for i in which) * piece
-        remote(tok.at[p, pl.ds(0, count)], tok_s.at[p], tok_r.at[p, g], partner).wait_recv()
+        remote(tok.at[p, pl.ds(0, count)], tok_s.at[p], tok_r.at[5 * p + g], partner).wait_recv()
 
     quarter = 2 * rows
     halves = 4 * rows
@@ -186,11 +187,11 @@
 
     def hid_send(b, r_at):
         sem = jnp.where((b == 0) & (r_at == r), 2, r_at)
-        return remote(hid_at(1, b, r_at), hid_s, hid_r.at[sem], outer, hid_at(0, b, r_at))
+        return remote(hid_at(1, b, r_at), z_s, gu_r.at[sem], outer, hid_at(0, b, r_at))
 
     def hid_wait(r_at, first, count, sem):
         held = hid.at[0, half_rows(r_at), pl.ds(first * lanes, count * lanes)]
-        remote(held, hid_s, hid_r.at[sem], partner).wait_recv()
+        remote(held, z_s, gu_r.at[sem], partner).wait_recv()
 
     def gated(p, b, r_at):
         both = jnp.dot(tok[p, half_rows(r_at), :], gu[b], preferred_element_type=jnp.float32)
@@ -201,17 +202,22 @@
     mid = sub // 2
     here, there = 0, 1
 
-    def pair_copy(p, side):
-        return remote(pair_out.at[p, side], pair_s, pair_r.at[p, side], partner, pair_in.at[p, side])
+    def pair_copy(at, side):
+        p = place(at)
+        return remote(pair_out.at[p, side], pair_s, pair_r.at[at % 4, side], partner, pair_in.at[p, side])
 
     def half_copy(p, way):
         return remote(
             half_out.at[p, way], half_s, half_r.at[p], along_y if way else along_x, half_in.at[p, way]
         )
 
-    def full_copy(p, way, part_at):
+    def full_sem(at):
+        return full_r.at[jnp.maximum(at - early + 1, 0)]
+
+    def full_copy(at, way, part_at):
+        p = place(at)
         return remote(
-            full_out.at[p, way, part_at], full_s, full_r.at[p], along_y if way else along_x, full_in.at[p, way, part_at]
+            full_out.at[p, way, part_at], full_s, full_sem(at), along_y if way else along_x, full_in.at[p, way, part_at]
         )
 
     def source(i):
@@ -227,7 +233,7 @@
         rows_at = half_rows(r_y if side == there else r)
         both = jnp.dot(hid[jnp.where(at < chunks, 0, 1), rows_at, :], dn[held], preferred_element_type=jnp.float32)
         pair_out[p, side] = both[quarter:].astype(jnp.bfloat16)
-        pair_copy(p, side).start()
+        pair_copy(at, side).start()
         kept[p, side] = both[:quarter]
 
     def send_own_gu():
@@ -267,10 +273,8 @@
                 go(0, 0, 1, 6, 7, 12, 13)
                 z_wait(0)
                 go(1, 0, 4)
-                got(0, 0, 1)
-                go(0, 14)
-                got(0, 6, 7)
-                go(0, 17)
+                got(0, 0, 1, 6, 7)
+                go(0, 14, 17)
                 z_wait(1)
                 go(1, 1, 5, 12)
                 got(1, 0, 4)
@@ -283,18 +287,14 @@
                 got(1, 6)
                 go(1, 10)
                 gu_pass(0, 0)
-                got(1, 7)
-                go(1, 17, 11)
-                got(1, 2, 3)
-                go(1, 15)
+                got(1, 2, 3, 7)
+                go(1, 17, 11, 15)
                 gu_pass(0, 1)
                 go(0, 2, 4)
                 gu_pass(1, 0)
                 go(0, 3, 5)
-                got(1, 8, 9)
-                go(1, 18)
-                got(1, 10, 11)
-                go(1, 19)
+                got(1, 8, 9, 10, 11)
+                go(1, 18, 19)
                 go(0, 8, 10)
                 gu_pass(1, 1)
                 got(1, 12, 13, 14, 15)
@@ -311,10 +311,8 @@
             @step(2)
             def _():
                 go(0, 9, 11)
-                got(0, 2, 3)
-                go(0, 15)
-                got(0, 4, 5)
-                go(0, 16)
+                got(0, 2, 3, 4, 5)
+                go(0, 15, 16)
                 gu_pass(2, 1)
 
             @pl.when(at_step == 2 + 4 * c)
@@ -332,10 +330,8 @@
 
             @step(6)
             def _():
-                got(0, 8, 9)
-                go(0, 18)
-                got(0, 10, 11)
-                go(0, 19)
+                got(0, 8, 9, 10, 11)
+                go(0, 18, 19)
                 gu_wait(2)
 
             @step(8)
@@ -371,7 +367,7 @@
 
     def finish_there(at):
         p = place(at)
-        pair_copy(p, there).wait_recv()
+        pair_copy(at, there).wait_recv()
         across = summed(p, there, 1 - x).astype(jnp.bfloat16)
         half_out[p, 0] = across[:, :mid]
         half_out[p, 1] = across[:, mid:]
@@ -380,42 +376,42 @@
         value = summed(p, there, x)
         kept[p, there, of(x), :mid] = value[:, :mid]
         full_out[p, 1, 1] = value[:, mid:].astype(jnp.bfloat16)
-        full_copy(p, 1, 1).start()
+        full_copy(at, 1, 1).start()
 
     def finish_here(at):
         p = place(at)
-        pair_copy(p, here).wait_recv()
+        pair_copy(at, here).wait_recv()
         value = summed(p, here, 1 - x)
         kept[p, here, of(1 - x), mid:] = value[:, mid:]
         full_out[p, 0, 0] = value[:, :mid].astype(jnp.bfloat16)
-        full_copy(p, 0, 0).start()
+        full_copy(at, 0, 0).start()
         fin[p] = summed(p, here, x)
 
-    across_copy = remote(diag_out, diag_s, diag_r, diag, diag_in)
+    across_copy = remote(diag_out, res_s, z_r.at[1], diag, diag_in)
 
     def finish_direct(at):
         p = place(at)
-        pair_copy(p, there).wait_recv()
+        pair_copy(at, there).wait_recv()
         diag_out[...] = summed(p, there, 1 - x).astype(jnp.bfloat16)
         across_copy.start()
         value = summed(p, there, x).astype(jnp.bfloat16)
         for part_at in (1, 0):
             full_out[p, 1, part_at] = value[:, part_at * mid : (part_at + 1) * mid]
-            full_copy(p, 1, part_at).start()
-        pair_copy(p, here).wait_recv()
+            full_copy(at, 1, part_at).start()
+        pair_copy(at, here).wait_recv()
         value = summed(p, here, 1 - x).astype(jnp.bfloat16)
         for part_at in (0, 1):
             full_out[p, 0, part_at] = value[:, part_at * mid : (part_at + 1) * mid]
-            full_copy(p, 0, part_at).start()
+            full_copy(at, 0, part_at).start()
         fin[p] = summed(p, here, x)
 
     def finish_half(at):
         p = place(at)
         remote(half_in.at[p], half_s, half_r.at[p], partner).wait_recv()
         full_out[p, 0, 1] = (kept[p, here, of(1 - x), mid:] + half_in[p, 1].astype(jnp.float32)).astype(jnp.bfloat16)
-        full_copy(p, 0, 1).start()
+        full_copy(at, 0, 1).start()
         full_out[p, 1, 0] = (kept[p, there, of(x), :mid] + half_in[p, 0].astype(jnp.float32)).astype(jnp.bfloat16)
-        full_copy(p, 1, 0).start()
+        full_copy(at, 1, 0).start()
 
     early = 2 * cuts
 
@@ -461,7 +457,7 @@
             pass_down(1, far_near, 1)
 
 
-    result = remote(res_out, res_s, res_r, outer, res_in)
+    result = remote(res_out, res_s, z_r.at[0], outer, res_in)
 
     def collect(at, part_at):
         p = place(at)
@@ -470,7 +466,7 @@
         return fin[p, :, cols] + both
 
     def arrive(at):
-        remote(full_in.at[place(at)], full_s, full_r.at[place(at)], along_x).wait_recv()
+        remote(full_in.at[place(at)], full_s, full_sem(at), along_x).wait_recv()
 
     def order(i):
         return jnp.where(in_middle & (i >= 2), jnp.where(i == 2, chunks, early + i - 1), early + i)
@@ -547,9 +543,9 @@
     def _():
         for p in (0, 1):
             total = sum(1 if i < 12 else 2 for i in range(len(sends))) * piece
-            remote(tok.at[p, pl.ds(0, total)], tok_s.at[p], tok_r.at[p, 0], partner).wait_send()
+            remote(tok.at[p, pl.ds(0, total)], tok_s.at[p], tok_r.at[p], partner).wait_send()
         remote(gu.at[:, pl.ds(0, depth)], gu_s.at[1], gu_r.at[0], inner).wait_send()
-        remote(hid.at[1], hid_s, hid_r.at[0], outer).wait_send()
+        remote(hid.at[1], z_s, gu_r.at[0], outer).wait_send()
         remote(dn.at[pl.ds(0, 2 * cuts)], dn_s.at[0], dn_r.at[0], inner).wait_send()
         remote(dn.at[pl.ds(0, 3 * cuts - 1)], dn_s.at[1], dn_r.at[0], outer).wait_send()
         remote(pair_out, pair_s, pair_r.at[0, 0], partner).wait_send()
@@ -563,9 +559,16 @@
 
     @pl.loop(0, chunks)
     def _(at):
+        @pl.when(at == 0)
+        def _():
+            remote(full_in.at[pl.ds(0, early)], full_s, full_sem(0), along_x).wait_recv()
+
+        @pl.when((at >= early) & (in_middle | (at < chunks - 2)))
+        def _():
+            arrive(at)
+
         @pl.when(in_middle | (at < chunks - 2))
         def _():
-            arrive(at)
             for part_at in (0, 1):
                 settle(at, part_at, collect(at, part_at))
 
@@ -646,22 +649,17 @@
             dma(()),
             dma((4,)),
             dma((2,)),
-            dma((2, 9)),
+            dma((12,)),
             dma((2,)),
             dma((3 * blocks,)),
             dma((2,)),
             dma((chunks,)),
             dma(()),
-            dma((3,)),
-            dma(()),
-            dma((chunks + 1, 2)),
+            dma((4, 2)),
             dma(()),
             dma((chunks + 1,)),
             dma(()),
-            dma((chunks + 1,)),
-            dma(()),
-            dma(()),
-            dma(()),
+            dma((chunks + 2 - 2 * cuts,)),
             dma(()),
         ],
         compiler_params=pltpu.CompilerParams(

time: 71 us -> 70.4 us (level)
  no operation moved by 1% of the time
where the time goes in v10:
time: 70.4 us; the launch traced here: 70.3 us
  Pallas kernels  69.5 us (99%)
  local copies, waits for them, and re-layouts  0.8 us (1%)
    pallas_call x1, Pallas kernels, chain_body(): pl.pallas_call(functools.partial(kernel, n, rows, depth, part, width, cut...  69.5 us

profile of v10, /device:TPU:0, one launch (start us, length us, event | category | flops | bytes accessed | tf_op | source)
XLA Modules:
  0.0 70.3 jit_solution(7903773234737891373)
XLA Ops:
  0.0 69.5 %shard_map.64 = bf16[128,2048]{1,0:T(8,128)(2,1)S(1)} custom-call(bf16[128,2048]{1,0:T(8,128)(2,1)} %tok_ref.1, f32[1,2048]{1,0:T(1,128)} %bitcast.2, bf16[512,768]{1,0:T(8,128)(2,1)} %wg_ref.1, bf16[512,768]{1,0:T(8,128)(2,1)} %wu_ref.1, bf16[768,512]{1,0:T(8,128)(2,1)} %wd_ref.1, f32[1,2048]{1,0:T(1,128)} %bitcast.3), custom_call_target="tpu_custom_call" | custom-call | tf_op jit(solution)/shard_map/pallas_call | solution.py:618
  69.5 0.8 %copy.8 = bf16[128,2048]{1,0:T(8,128)(2,1)} copy(bf16[128,2048]{1,0:T(8,128)(2,1)S(1)} %shard_map.64) | data formatting | bytes 1048576

commit v11 on v10

--- a/solution.py
+++ b/solution.py
@@ -78,7 +78,7 @@
     gain_load.start()
 
     barrier = pltpu.get_barrier_semaphore()
-    for where in (partner, along_x, along_y, diag, inner):
+    for where in (partner, along_x, along_y, inner):
         pl.semaphore_signal(barrier, inc=1, device_id=where, device_id_type=MESH)
 
     @pl.when(in_middle)
@@ -103,7 +103,7 @@
         to = pl.ds(pl.multiple_of(first + i * tile, tile), tile)
         tok[0, to, :] = rms_scale(raw[at, :].astype(jnp.float32), gain[...]).astype(jnp.bfloat16)
 
-    pl.semaphore_wait(barrier, 5 + jnp.where(in_middle, 1, 0))
+    pl.semaphore_wait(barrier, 4 + jnp.where(in_middle, 1, 0))
 
     def remote(ref, send, recv, where, to=None):
         return pltpu.make_async_remote_copy(

time: 70.4 us -> 70.4 us (level)
  no operation moved by 1% of the time
where the time goes in v11:
time: 70.4 us; the launch traced here: 70.3 us
  Pallas kernels  69.5 us (99%)
  local copies, waits for them, and re-layouts  0.8 us (1%)
    pallas_call x1, Pallas kernels, chain_body(): pl.pallas_call(functools.partial(kernel, n, rows, depth, part, width, cut...  69.5 us

profile of v11, /device:TPU:0, one launch (start us, length us, event | category | flops | bytes accessed | tf_op | source)
XLA Modules:
  0.0 70.3 jit_solution(113638842812497625)
XLA Ops:
  0.0 69.5 %shard_map.64 = bf16[128,2048]{1,0:T(8,128)(2,1)S(1)} custom-call(bf16[128,2048]{1,0:T(8,128)(2,1)} %tok_ref.1, f32[1,2048]{1,0:T(1,128)} %bitcast.2, bf16[512,768]{1,0:T(8,128)(2,1)} %wg_ref.1, bf16[512,768]{1,0:T(8,128)(2,1)} %wu_ref.1, bf16[768,512]{1,0:T(8,128)(2,1)} %wd_ref.1, f32[1,2048]{1,0:T(1,128)} %bitcast.3), custom_call_target="tpu_custom_call" | custom-call | tf_op jit(solution)/shard_map/pallas_call | solution.py:618
  69.5 0.8 %copy.8 = bf16[128,2048]{1,0:T(8,128)(2,1)} copy(bf16[128,2048]{1,0:T(8,128)(2,1)S(1)} %shard_map.64) | data formatting | bytes 1048576
